TPU v7x, 32 devices: a whole 2x2x4 slice. The times are simulated.
32 devices in a mesh: sp: 8 (over z, y), tp: 4 (over x, core).
Axes of the slice: x: 2, y: 2, z: 4, core: 2. Of those that a mesh axis runs over, the one named last changes fastest.
Arguments:
- conv_input: bfloat16 [4096, 1024], P('sp', 'tp'), may hold values from -6 to 6
- gate_inner: bfloat16 [4096, 1024], P('sp', 'tp'), may hold values from -6 to 6
- gate_outer: bfloat16 [4096, 1024], P('sp', 'tp'), may hold values from -6 to 6
- conv_taps: bfloat16 [3, 1024], P(None, 'tp'), may hold values from -3.5 to 3.5
- doc_ids: int32 [4096], P('sp'), may hold values from 0 to 3, never falling along the last dimension, each value on 1 to 2048 neighbouring positions
- residual_in: bfloat16 [4096, 2048], P(('sp', 'tp')), may hold values from -6 to 6
- out_proj: bfloat16 [1024, 2048], replicated, may hold values from -0.1875 to 0.1875
- norm_gain: float32 [2048], replicated, may hold values from 0.1 to 1.9
- expert_ids: int32 [4096, 2], P(('sp', 'tp')), may hold values from 0 to 31, all different within a row; in each aligned block of 128 rows (0 to 127, 128 to 255, ...) at most 16 rows name the same one
- expert_weights: float32 [4096, 2], P(('sp', 'tp')), may hold values from 0.2 to 1
- gate_proj: bfloat16 [32, 2048, 1024], P(('sp', 'tp')), may hold values from -0.125 to 0.125
- up_proj: bfloat16 [32, 2048, 1024], P(('sp', 'tp')), may hold values from -0.125 to 0.125
- down_proj: bfloat16 [32, 1024, 2048], P(('sp', 'tp')), may hold values from -0.1875 to 0.1875
Outputs:
- layer_out: bfloat16 [4096, 2048], P(('sp', 'tp'))
Inputs may be any that keep to these rules, and one draw needn't show every extreme that they name: `doc_ids`: never falls along positions; each document has at most 2048 positions. `expert_ids`: each row names 2 different experts; within the rows of one device, aligned blocks of 128 rows, no expert is named more than 16 times, a bound that some block reaches.
All inputs are finite; a program needn't handle non-finite values.
Results may differ from a plain program's by a relative error of at most 0.009.
Values may be sent and summed in bfloat16 or wider, within the bound.
A program may use at most 64 MiB of HBM per device.

v0:
```python
import functools

import jax
import jax.numpy as jnp
from jax import lax
from jax.experimental import pallas as pl
from jax.experimental.pallas import tpu as pltpu
from jax.sharding import PartitionSpec as P

MESH = pl.DeviceIdType.MESH


def layer_kernel(
    sp_count, tp_count, cap, pieces,
    conv_ref, inner_ref, outer_ref, taps_ref, docs_ref, residual_ref, gain_ref,
    meta_ref, gate_hbm, up_hbm, down_hbm, proj_hbm,
    out_ref,
    x_ref, carried_ref, proj_w, padded, padded_docs, tail, tail_in, conv_out, conv_in,
    gate_w, up_w, down_w, meta_far, x_far, slots, arrived, hidden, served, back, part_out, part_in,
    w_sem, tail_sem, conv_send, conv_recv, meta_sem, dense_send, dense_recv, part_send, part_recv, go_send, go_recv, ret_send, ret_recv,
):
    sp = lax.axis_index("sp")
    tp = lax.axis_index("tp")
    half = sp_count // 2
    group = half * tp_count
    base = lax.div(sp, half) * half
    mine = (sp - base) * tp_count + tp
    far = (lax.rem(sp + half, sp_count), tp)
    rows, width = x_ref.shape
    step = width // pieces
    ff = gate_w.shape[1]
    tile = 256
    slot_count = group * cap

    def where(member):
        return (base + lax.div(member, tp_count), lax.rem(member, tp_count))

    def peer(i):
        odd = lax.rem(i, 2)
        shift = group // 2 + (1 - 2 * odd) * lax.div(i + 1, 2)
        return lax.rem(mine + shift, group)

    pairs = ((gate_hbm.at[0], gate_w), (up_hbm.at[0], up_w), (down_hbm.at[0], down_w), (proj_hbm, proj_w))
    loads = [
        pltpu.make_async_copy(source, target, w_sem.at[n])
        for n, (source, target) in enumerate(pairs)
    ]
    for load in loads[3:] + loads[:3]:
        load.start()

    barrier = pltpu.get_barrier_semaphore()
    pl.semaphore_signal(barrier, inc=1, device_id=far, device_id_type=MESH)

    @pl.loop(0, group - 1)
    def _(i):
        pl.semaphore_signal(barrier, inc=1, device_id=where(peer(i)), device_id_type=MESH)

    after = (lax.rem(sp + 1, sp_count), tp)
    before = (lax.rem(sp + sp_count - 1, sp_count), tp)
    for neighbour in (after, before):
        pl.semaphore_signal(barrier, inc=1, device_id=neighbour, device_id_type=MESH)

    length, channels = conv_ref.shape
    lanes = docs_ref.shape[1]
    edge = tail.shape[0]
    padded[edge:, :] = conv_ref[...].astype(jnp.float32) * inner_ref[...].astype(jnp.float32)
    padded_docs[edge:, :] = docs_ref[...]
    tail[:, :channels] = padded[length:, :]
    tail[:, channels:] = padded_docs[length:, :]
    pl.semaphore_wait(barrier, group + 2)

    tail_copy = pltpu.make_async_remote_copy(
        src_ref=tail, dst_ref=tail_in, send_sem=tail_sem.at[0], recv_sem=tail_sem.at[1],
        device_id=after, device_id_type=MESH,
    )
    tail_copy.start()
    tail_copy.wait()
    padded[:edge, :] = tail_in[:, :channels]
    padded_docs[:edge, :] = jnp.where(sp == 0, -1.0, tail_in[:, channels:])
    docs = docs_ref[...]
    same_one = padded_docs[edge - 1 : edge - 1 + length, :] == docs
    same_two = padded_docs[edge - 2 : edge - 2 + length, :] == docs
    taps = taps_ref[...].astype(jnp.float32)
    for k in range(channels // lanes):
        at = slice(k * lanes, (k + 1) * lanes)
        one_back = jnp.where(same_one, padded[edge - 1 : edge - 1 + length, at], 0.0)
        two_back = jnp.where(same_two, padded[edge - 2 : edge - 2 + length, at], 0.0)
        mixed = taps[2:3, at] * padded[edge:, at] + taps[1:2, at] * one_back + taps[0:1, at] * two_back
        gated = (outer_ref[:, at].astype(jnp.float32) * mixed).astype(jnp.bfloat16)
        conv_out[:, :, at] = gated.reshape(tp_count, rows, lanes)

    def conv_copy(other, landing):
        return pltpu.make_async_remote_copy(
            src_ref=conv_out.at[other], dst_ref=conv_in.at[landing],
            send_sem=conv_send.at[other], recv_sem=conv_recv.at[landing],
            device_id=(sp, other), device_id_type=MESH,
        )

    others = [lax.rem(tp + j, tp_count) for j in range(1, tp_count)]
    for other in others:
        conv_copy(other, tp).start()
    conv_in[pl.ds(tp, 1)] = conv_out[pl.ds(tp, 1)]
    loads[3].wait()
    for other in others:
        conv_copy(other, other).wait_recv()
    for c in range(pieces):
        at = slice(c * step, (c + 1) * step)
        mix = jnp.zeros((rows, step), jnp.float32)
        for j in range(tp_count):
            lines = slice(j * channels, (j + 1) * channels)
            mix += jnp.dot(conv_in[j], proj_w[lines, at], preferred_element_type=jnp.float32)
        carried_ref[:, at] = residual_ref[:, at].astype(jnp.float32) + mix.astype(jnp.bfloat16).astype(jnp.float32)
    carried = carried_ref[...]
    scale = lax.rsqrt(jnp.mean(carried * carried, axis=1, keepdims=True) + 1e-06)
    x_ref[...] = (carried * scale * gain_ref[...]).astype(jnp.bfloat16)

    def dense_copy(c):
        return pltpu.make_async_remote_copy(
            src_ref=x_ref.at[:, pl.ds(c * step, step)], dst_ref=x_far.at[c],
            send_sem=dense_send.at[c], recv_sem=dense_recv.at[c], device_id=far, device_id_type=MESH,
        )

    def part_copy(c):
        return pltpu.make_async_remote_copy(
            src_ref=part_out.at[c], dst_ref=part_in.at[c],
            send_sem=part_send.at[c], recv_sem=part_recv.at[c], device_id=far, device_id_type=MESH,
        )

    def exchange(source, target, send, recv, p, c, other, landing):
        return pltpu.make_async_remote_copy(
            src_ref=source.at[p, c, other], dst_ref=target.at[p, c, landing],
            send_sem=send.at[p, c, other], recv_sem=recv.at[p, c, landing],
            device_id=where(other), device_id_type=MESH,
        )

    def send_all(source, target, send, recv, p, c):
        @pl.loop(0, group - 1)
        def _(i):
            exchange(source, target, send, recv, p, c, peer(i), mine).start()

        target[p, c, pl.ds(mine, 1)] = source[p, c, pl.ds(mine, 1)]

    def wait_all(source, target, send, recv, p, c):
        @pl.loop(0, group - 1)
        def _(i):
            other = peer(i)
            exchange(source, target, send, recv, p, c, other, other).wait_recv()

    def wait_sent(source, target, send, recv):
        for p in range(2):
            @pl.loop(0, pieces)
            def _(c):
                @pl.loop(0, group - 1)
                def _(i):
                    other = peer(i)
                    exchange(source, target, send, recv, p, c, other, other).wait_send()

    go = (slots, arrived, go_send, go_recv)
    ret = (served, back, ret_send, ret_recv)

    meta_copy = pltpu.make_async_remote_copy(
        src_ref=meta_ref, dst_ref=meta_far, send_sem=meta_sem.at[0], recv_sem=meta_sem.at[1],
        device_id=far, device_id_type=MESH,
    )
    meta_copy.start()

    def matches(meta):
        first = base * tp_count * cap
        ids = (lax.broadcasted_iota(jnp.int32, (slot_count, rows), 0) + first).astype(jnp.float32)
        choices = meta.shape[0] // 2
        return [(meta[k : k + 1, :] == ids, meta[choices + k : choices + k + 1, :]) for k in range(choices)]

    def placing(meta):
        total = jnp.zeros((slot_count, rows), jnp.float32)
        for hit, _ in matches(meta):
            total = total + jnp.where(hit, 1.0, 0.0)
        return total.astype(jnp.bfloat16)

    def weighing(meta):
        total = jnp.zeros((slot_count, rows), jnp.float32)
        for hit, weight in matches(meta):
            total = total + jnp.where(hit, weight, 0.0)
        total = total.T
        high = total.astype(jnp.bfloat16)
        return high, (total - high.astype(jnp.float32)).astype(jnp.bfloat16)

    def fill(p, c, place, block):
        picked = jnp.dot(place, block, preferred_element_type=jnp.float32).astype(jnp.bfloat16)
        slots[p, c] = picked.reshape(group, cap, step)
        send_all(*go, p, c)

    place = placing(meta_ref[...])
    for c in range(pieces):
        dense_copy(c).start()
        fill(0, c, place, x_ref[:, c * step : (c + 1) * step])

    meta_copy.wait()
    place = placing(meta_far[...])
    for c in range(pieces):
        dense_copy(c).wait_recv()
        fill(1, c, place, x_far[c])

    for p in range(2):
        for c in range(pieces):
            wait_all(*go, p, c)
        if p == 0:
            loads[0].wait()
            loads[1].wait()

        @pl.loop(0, ff // tile)
        def _(f):
            columns = pl.ds(pl.multiple_of(f * tile, tile), tile)
            gate_value = jnp.zeros((slot_count, tile), jnp.float32)
            up_value = jnp.zeros((slot_count, tile), jnp.float32)
            for c in range(pieces):
                piece = arrived[p, c].reshape(slot_count, step)
                lines = pl.ds(c * step, step)
                gate_value += jnp.dot(piece, gate_w[lines, columns], preferred_element_type=jnp.float32)
                up_value += jnp.dot(piece, up_w[lines, columns], preferred_element_type=jnp.float32)
            silu = gate_value * (1.0 / (1.0 + jnp.exp(-gate_value)))
            hidden[:, columns] = (silu * up_value).astype(jnp.bfloat16)

        if p == 0:
            loads[2].wait()

        for c in range(pieces):
            value = jnp.dot(
                hidden[...], down_w[:, c * step : (c + 1) * step], preferred_element_type=jnp.float32
            ).astype(jnp.bfloat16)
            served[p, c] = value.reshape(group, cap, step)
            send_all(*ret, p, c)

    def weighted(p, c, high, low):
        got = back[p, c].reshape(slot_count, step)
        return jnp.dot(high, got, preferred_element_type=jnp.float32) + jnp.dot(
            low, got, preferred_element_type=jnp.float32
        )

    high, low = weighing(meta_far[...])
    for c in range(pieces):
        wait_all(*ret, 1, c)
        part_out[c] = weighted(1, c, high, low).astype(jnp.bfloat16)
        part_copy(c).start()
    high, low = weighing(meta_ref[...])
    for c in range(pieces):
        wait_all(*ret, 0, c)
        total = carried_ref[:, c * step : (c + 1) * step] + weighted(0, c, high, low)
        part_copy(c).wait_recv()
        out_ref[:, c * step : (c + 1) * step] = (total + part_in[c].astype(jnp.float32)).astype(jnp.bfloat16)

    for other in others:
        conv_copy(other, other).wait_send()
    for c in range(pieces):
        dense_copy(c).wait_send()
        part_copy(c).wait_send()
    wait_sent(*go)
    wait_sent(*ret)


def run_layer(front, meta, gate_proj, up_proj, down_proj, out_proj, cap, pieces=2):
    sp_count, tp_count = lax.axis_size("sp"), lax.axis_size("tp")
    length, channels = front[0].shape
    lanes = front[4].shape[1]
    rows, width = front[5].shape
    edge = 8
    ff = gate_proj.shape[2]
    group = sp_count // 2 * tp_count
    step = width // pieces
    slot_shape = (2, pieces, group, cap, step)
    dma = pltpu.SemaphoreType.DMA
    vmem = pl.BlockSpec(memory_space=pltpu.VMEM)
    hbm = pl.BlockSpec(memory_space=pl.ANY)
    return pl.pallas_call(
        functools.partial(layer_kernel, sp_count, tp_count, cap, pieces),
        out_shape=jax.ShapeDtypeStruct((rows, width), jnp.bfloat16),
        in_specs=[vmem] * 8 + [hbm] * 4,
        out_specs=vmem,
        scratch_shapes=[
            pltpu.VMEM((rows, width), jnp.bfloat16),
            pltpu.VMEM((rows, width), jnp.float32),
            pltpu.VMEM(out_proj.shape, jnp.bfloat16),
            pltpu.VMEM((edge + length, channels), jnp.float32),
            pltpu.VMEM((edge + length, lanes), jnp.float32),
            pltpu.VMEM((edge, channels + lanes), jnp.float32),
            pltpu.VMEM((edge, channels + lanes), jnp.float32),
            pltpu.VMEM((tp_count, rows, channels), jnp.bfloat16),
            pltpu.VMEM((tp_count, rows, channels), jnp.bfloat16),
            pltpu.VMEM((width, ff), jnp.bfloat16),
            pltpu.VMEM((width, ff), jnp.bfloat16),
            pltpu.VMEM((ff, width), jnp.bfloat16),
            pltpu.VMEM(meta.shape, jnp.float32),
            pltpu.VMEM((pieces, rows, step), jnp.bfloat16),
            pltpu.VMEM(slot_shape, jnp.bfloat16),
            pltpu.VMEM(slot_shape, jnp.bfloat16),
            pltpu.VMEM((group * cap, ff), jnp.bfloat16),
            pltpu.VMEM(slot_shape, jnp.bfloat16),
            pltpu.VMEM(slot_shape, jnp.bfloat16),
            pltpu.VMEM((pieces, rows, step), jnp.bfloat16),
            pltpu.VMEM((pieces, rows, step), jnp.bfloat16),
            dma((4,)),
            dma((2,)),
            dma((tp_count,)),
            dma((tp_count,)),
            dma((2,)),
            dma((pieces,)),
            dma((pieces,)),
            dma((pieces,)),
            dma((pieces,)),
            dma((2, pieces, group)),
            dma((2, pieces, group)),
            dma((2, pieces, group)),
            dma((2, pieces, group)),
        ],
        compiler_params=pltpu.CompilerParams(
            collective_id=0, has_side_effects=True, vmem_limit_bytes=48 * 1024 * 1024
        ),
    )(*front, meta, gate_proj, up_proj, down_proj, out_proj)


def from_behind(block, axis, distance):
    devices = range(lax.axis_size(axis))
    route = [(i - distance, i) for i in devices if i - distance in devices]
    return lax.ppermute(block, axis, route)


def expert_rows(arrived, gate_weight, up_weight, down_weight):
    gate_value = jnp.dot(arrived, gate_weight, preferred_element_type=jnp.float32)
    up_value = jnp.dot(arrived, up_weight, preferred_element_type=jnp.float32)
    hidden = (jax.nn.silu(gate_value) * up_value).astype(jnp.bfloat16)
    return jnp.dot(hidden, down_weight, preferred_element_type=jnp.float32).astype(jnp.bfloat16)


def on_device(
    conv_input,
    gate_inner,
    gate_outer,
    conv_taps,
    doc_ids,
    residual_in,
    out_proj,
    norm_gain,
    expert_ids,
    expert_weights,
    gate_proj,
    up_proj,
    down_proj,
):
    inner_prod = conv_input.astype(jnp.float32) * gate_inner.astype(jnp.float32)
    earlier, earlier_docs = from_behind((inner_prod[-2:], doc_ids[-2:]), "sp", 1)
    padded = jnp.concatenate([earlier, inner_prod], axis=0)
    padded_docs = jnp.concatenate([earlier_docs, doc_ids], axis=0)
    length = inner_prod.shape[0]
    tap_values = conv_taps.astype(jnp.float32)
    one_back = jnp.where(
        (padded_docs[1 : length + 1] == doc_ids)[:, None], padded[1 : length + 1], 0.0
    )
    two_back = jnp.where((padded_docs[:length] == doc_ids)[:, None], padded[:length], 0.0)
    mixed_rows = tap_values[2] * inner_prod + tap_values[1] * one_back + tap_values[0] * two_back
    conv_out = (gate_outer.astype(jnp.float32) * mixed_rows).astype(jnp.bfloat16)
    row_count = residual_in.shape[0]
    regrouped = lax.all_to_all(conv_out, "tp", split_axis=0, concat_axis=1, tiled=True)
    mix = jnp.dot(regrouped, out_proj, preferred_element_type=jnp.float32).astype(jnp.bfloat16)
    carried = residual_in.astype(jnp.float32) + mix.astype(jnp.float32)
    normed = (
        carried * lax.rsqrt(jnp.mean(carried * carried, axis=1, keepdims=True) + 1e-06) * norm_gain
    ).astype(jnp.bfloat16)
    model_width = normed.shape[1]
    choose = expert_ids.shape[1]
    sp_count = lax.axis_size("sp")
    tp_count = lax.axis_size("tp")
    experts_total = sp_count * tp_count
    capacity = 2 * row_count * choose // experts_total
    flat_ids = expert_ids.reshape(-1)
    onehot = (flat_ids[:, None] == jnp.arange(experts_total, dtype=jnp.int32)[None, :]).astype(
        jnp.int32
    )
    slot_rank = jnp.sum((jnp.cumsum(onehot, axis=0) - 1) * onehot, axis=1)
    target = flat_ids * capacity + slot_rank
    if capacity % 16 == 0 and sp_count % 2 == 0:
        places = target.reshape(row_count, choose).astype(jnp.float32)
        meta = jnp.concatenate([places.T, expert_weights.T], axis=0)
        docs = jnp.broadcast_to(doc_ids.astype(jnp.float32)[:, None], (doc_ids.shape[0], 128))
        front = (conv_input, gate_inner, gate_outer, conv_taps, docs, residual_in, norm_gain[None, :])
        return run_layer(front, meta, gate_proj, up_proj, down_proj, out_proj, capacity)
    sources = jnp.repeat(normed, choose, axis=0)
    outgoing = (
        jnp.zeros((experts_total * capacity, model_width), jnp.bfloat16).at[target].set(sources)
    )
    gate_weight = gate_proj[0]
    up_weight = up_proj[0]
    down_weight = down_proj[0]
    arrived = lax.all_to_all(
        outgoing.reshape(experts_total, capacity, model_width),
        ("sp", "tp"),
        split_axis=0,
        concat_axis=0,
        tiled=True,
    )
    item_count = arrived.shape[1]
    flat_rows = arrived.reshape(-1, model_width)
    result = expert_rows(flat_rows, gate_weight, up_weight, down_weight)
    result = result.reshape(experts_total, item_count, model_width)
    returned = lax.all_to_all(result, ("sp", "tp"), split_axis=0, concat_axis=0, tiled=True)
    picked = (
        returned.reshape(-1, model_width)[target]
        .reshape(row_count, choose, model_width)
        .astype(jnp.float32)
    )
    combined = carried + jnp.sum(expert_weights[:, :, None] * picked, axis=1)
    return combined.astype(jnp.bfloat16)


def solution(mesh):
    in_specs = (
        P("sp", "tp"),
        P("sp", "tp"),
        P("sp", "tp"),
        P(None, "tp"),
        P("sp"),
        P(("sp", "tp"), None),
        P(),
        P(),
        P(("sp", "tp"), None),
        P(("sp", "tp"), None),
        P(("sp", "tp"), None, None),
        P(("sp", "tp"), None, None),
        P(("sp", "tp"), None, None),
    )
    out_specs = P(("sp", "tp"), None)
    return jax.shard_map(
        on_device, mesh=mesh, in_specs=in_specs, out_specs=out_specs, check_vma=False
    )
```

profile of v0, /device:TPU:0, one launch (start us, length us, event | category | flops | bytes accessed | tf_op | source)
XLA Modules:
  0.0 107.6 jit_solution(18279076037329368788)
XLA Ops:
  0.0 0.7 convert_element_type.11
  0.7 0.8 copy.14
  1.5 0.1 eq.29
  1.6 0.1 eq.25
  1.8 0.6 reduce-window.6
  2.4 0.2 slice_reduce_fusion
  2.6 0.1 fusion.1
  2.7 0.1 reduce_sum.12
  2.8 0.1 copy.17
  2.9 0.7 convert_bitcast_fusion
  3.6 0.7 pad_maximum_fusion.meta_ref
  4.3 0.1 broadcast_in_dim.4.docs_ref
  4.4 0.0 copy-start
  4.4 1.0 copy-done
  5.5 0.0 copy-start.1
  5.5 0.9 copy-done.1
  6.4 0.9 copy-done.2
  7.4 0.0 copy-start.3
  7.4 0.9 copy-done.3
  8.3 0.0 copy-start.4
  8.3 0.7 copy-done.4
  9.0 0.7 copy-done.5
  9.7 97.1 %shard_map.127 = bf16[128,2048]{1,0:T(8,128)(2,1)S(1)} custom-call(bf16[512,256]{1,0:T(8,128)(2,1)S(1)} %copy-done.1, bf16[512,256]{1,0:T(8,128)(2,1)S(1)} %copy-done.2, bf16[512,256]{1,0:T(8,128)(2,1)S(1)} %copy-done.3, bf16[3,256]{1,0:T(4,128)(2,1)S(1)} %copy-done.5, f32[512,128]{1,0:T(8,128)S(1)} %broadcast_in_dim.4.docs_ref, ...), custom_call_target="tpu_custom_call" | custom-call | tf_op jit(solution)/shard_map/pallas_call | solution.py:273
  106.8 0.8 copy.21
  (5 shorter events, 0.1 us)
Async XLA Ops:
  4.4 1.0 copy-start
  5.5 0.9 copy-start.1
  6.4 0.9 copy-start.2
  7.4 0.9 copy-start.3
  8.3 0.7 copy-start.4
  9.0 0.7 copy-start.5
where the time goes:
time: 108 us
  Pallas kernels  97.1 us (90%)
  local copies, waits for them, and re-layouts  7.63 us (7%)
  other arithmetic  2.81 us (3%)
    pallas_call x1, Pallas kernels, run_layer(): pl.pallas_call(functools.partial(layer_kernel, sp_count, tp_count, cap, p...  97.1 us
    unnamed x14, local copies, waits for them, and re-layouts  6.85 us

commit v1 on v0

v1 whole, which is shorter than its diff:
```python
import functools

import jax
import jax.numpy as jnp
from jax import lax
from jax.experimental import pallas as pl
from jax.experimental.pallas import tpu as pltpu
from jax.sharding import PartitionSpec as P

MESH = pl.DeviceIdType.MESH
DEPTH = 4


def layer_kernel(
    sp_count, tp_count, cap, pieces,
    conv_hbm, inner_hbm, outer_hbm, taps_hbm, docs_hbm, residual_hbm, gain_hbm, ids_hbm, scores_hbm,
    gate_hbm, up_hbm, down_hbm, proj_hbm,
    out_ref,
    conv_ref, inner_ref, outer_ref, taps_ref, docs_ref, residual_ref, gain_ref, ids_ref, scores_ref,
    gate_w, up_w, down_w, proj_w,
    padded, padded_docs, tail, tail_in, conv_out, conv_in, carried_ref,
    metas, place, wide, high, low, x_all, slots, arrived, served, back, hidden, sums, held, part_out, part_in,
    load_sem, tail_sem, conv_send, conv_recv, meta_send, meta_recv, x_send, x_recv,
    go_send, go_recv, ret_send, ret_recv, part_send, part_recv,
):
    sp = lax.axis_index("sp")
    tp = lax.axis_index("tp")
    span = sp_count // DEPTH
    group = span * tp_count
    z = lax.div(sp, span)
    y = lax.rem(sp, span)
    mine = y * tp_count + tp
    rows, width = carried_ref.shape
    step = width // pieces
    ff = gate_w.shape[1]
    slot_count = group * cap

    low_half = 1 - lax.div(z, DEPTH // 2)
    top = DEPTH - 1
    inward = z * low_half + (top - z) * (1 - low_half)
    is_end = inward == 0

    def flip(k):
        return k * low_half + (top - k) * (1 - low_half)

    def source(end, middle):
        return flip(end * (1 - inward) + middle * inward)

    order = (source(2, 0), source(3, 2), source(1, 3))
    outer_z, inner_z = flip(inward - 1), flip(inward + 1)

    def peer(i):
        return lax.rem(mine + i, group)

    def where(member):
        return (z * span + lax.div(member, tp_count), lax.rem(member, tp_count))

    def along(level):
        return (level * span + y, tp)

    peers = [peer(group - 1 - i) for i in range(group - 1)]
    homes = [where(other) for other in peers]

    pairs = (
        (conv_hbm, conv_ref), (inner_hbm, inner_ref), (docs_hbm, docs_ref), (taps_hbm, taps_ref), (outer_hbm, outer_ref),
        (ids_hbm, ids_ref), (scores_hbm, scores_ref), (residual_hbm, residual_ref), (gain_hbm, gain_ref),
        (proj_hbm, proj_w), (gate_hbm.at[0], gate_w), (up_hbm.at[0], up_w), (down_hbm.at[0], down_w),
    )
    loads = [
        pltpu.make_async_copy(origin, target, load_sem.at[n]) for n, (origin, target) in enumerate(pairs)
    ]
    for load in loads:
        load.start()

    barrier = pltpu.get_barrier_semaphore()
    for home in homes:
        pl.semaphore_signal(barrier, inc=1, device_id=home, device_id_type=MESH)
    levels = [lax.rem(z + i, DEPTH) for i in range(1, DEPTH)]
    for level in levels:
        pl.semaphore_signal(barrier, inc=1, device_id=along(level), device_id_type=MESH)

    @pl.when(sp < sp_count - 1)
    def _():
        pl.semaphore_signal(barrier, inc=1, device_id=(sp + 1, tp), device_id_type=MESH)

    @pl.when(sp > 0)
    def _():
        pl.semaphore_signal(barrier, inc=1, device_id=(sp - 1, tp), device_id_type=MESH)

    length, channels = conv_ref.shape
    lanes = tail.shape[1] - channels
    edge = tail.shape[0]
    for load in loads[:3]:
        load.wait()
    padded[edge:, :] = conv_ref[...].astype(jnp.float32) * inner_ref[...].astype(jnp.float32)
    docs = docs_ref[...].astype(jnp.float32)
    for j in range(length // lanes):
        at = slice(edge + j * lanes, edge + (j + 1) * lanes)
        padded_docs[at, :] = jnp.broadcast_to(docs[j : j + 1, :], (lanes, lanes)).T
    tail[:, :channels] = padded[length:, :]
    tail[:, channels:] = padded_docs[length:, :]
    for load in loads[3:5]:
        load.wait()
    taps = taps_ref[...].astype(jnp.float32)

    def convolve(b):
        first = edge + b * rows
        docs = padded_docs[first : first + rows, :]
        same_one = padded_docs[first - 1 : first - 1 + rows, :] == docs
        same_two = padded_docs[first - 2 : first - 2 + rows, :] == docs
        for k in range(channels // lanes):
            at = slice(k * lanes, (k + 1) * lanes)
            one_back = jnp.where(same_one, padded[first - 1 : first - 1 + rows, at], 0.0)
            two_back = jnp.where(same_two, padded[first - 2 : first - 2 + rows, at], 0.0)
            here = padded[first : first + rows, at]
            mixed = taps[2:3, at] * here + taps[1:2, at] * one_back + taps[0:1, at] * two_back
            gated = outer_ref[b * rows : (b + 1) * rows, at].astype(jnp.float32) * mixed
            conv_out[b, :, at] = gated.astype(jnp.bfloat16)

    def conv_copy(b, landing):
        return pltpu.make_async_remote_copy(
            src_ref=conv_out.at[b], dst_ref=conv_in.at[landing],
            send_sem=conv_send.at[b], recv_sem=conv_recv.at[landing],
            device_id=(sp, b), device_id_type=MESH,
        )

    def hand_out(b):
        @pl.when(tp != b)
        def _():
            conv_copy(b, tp).start()

        @pl.when(tp == b)
        def _():
            conv_in[b] = conv_out[b]

    for b in range(1, tp_count):
        convolve(b)
    for load in loads[5:7]:
        load.wait()
    metas.at[z][0:2, :] = ids_ref[...].astype(jnp.float32)
    metas.at[z][2:4, :] = scores_ref[...]
    metas.at[z][4:, :] = jnp.zeros((4, rows), jnp.float32)

    behind = lax.div(sp + sp_count - 1, sp_count)
    ahead = lax.div(2 * sp_count - 2 - sp, sp_count)
    pl.semaphore_wait(barrier, group - 1 + DEPTH - 1 + behind + ahead)

    tail_copy = pltpu.make_async_remote_copy(
        src_ref=tail, dst_ref=tail_in, send_sem=tail_sem.at[0], recv_sem=tail_sem.at[1],
        device_id=(lax.rem(sp + 1, sp_count), tp), device_id_type=MESH,
    )

    @pl.when(sp < sp_count - 1)
    def _():
        tail_copy.start()

    for b in range(1, tp_count):
        hand_out(b)

    def meta_copy(i):
        return pltpu.make_async_remote_copy(
            src_ref=metas.at[z], dst_ref=metas.at[z], send_sem=meta_send.at[i], recv_sem=meta_recv.at[z],
            device_id=along(levels[i]), device_id_type=MESH,
        )

    def meta_arrival(i):
        return pltpu.make_async_remote_copy(
            src_ref=metas.at[levels[i]], dst_ref=metas.at[levels[i]],
            send_sem=meta_send.at[i], recv_sem=meta_recv.at[levels[i]],
            device_id=along(levels[i]), device_id_type=MESH,
        )

    for i in range(DEPTH - 1):
        meta_copy(i).start()

    first_expert = (z * group).astype(jnp.float32)
    ids = lax.broadcasted_iota(jnp.int32, (group, rows), 0).astype(jnp.float32) + first_expert
    earlier = lax.broadcasted_iota(jnp.int32, (rows, rows), 0) < lax.broadcasted_iota(jnp.int32, (rows, rows), 1)
    earlier = jnp.where(earlier, 1.0, 0.0).astype(jnp.bfloat16)
    seats = lax.broadcasted_iota(jnp.int32, (cap, rows), 0).astype(jnp.float32)

    def choose(s):
        meta = metas.at[s][...]
        taken = jnp.zeros((group, rows), jnp.float32)
        weight = jnp.zeros((group, rows), jnp.float32)
        for k in range(2):
            hit = meta[k : k + 1, :] == ids
            taken = taken + jnp.where(hit, 1.0, 0.0)
            weight = weight + jnp.where(hit, meta[2 + k : 3 + k, :], 0.0)
        rank = jnp.dot(taken.astype(jnp.bfloat16), earlier, preferred_element_type=jnp.float32)
        rank = jnp.where(taken > 0.5, rank, -1.0)
        for e in range(group):
            at = slice(e * cap, (e + 1) * cap)
            seated = rank[e : e + 1, :] == seats
            place.at[s][at, :] = jnp.where(seated, 1.0, 0.0).astype(jnp.bfloat16)
            wide[at, :] = jnp.where(seated, weight[e : e + 1, :], 0.0)
        total = wide[...].T
        upper = total.astype(jnp.bfloat16)
        high.at[s][...] = upper
        low.at[s][...] = (total - upper.astype(jnp.float32)).astype(jnp.bfloat16)

    choose(z)

    @pl.when(sp == 0)
    def _():
        tail_in[:, :channels] = jnp.zeros((edge, channels), jnp.float32)
        tail_in[:, channels:] = jnp.full((edge, lanes), -1.0, jnp.float32)

    @pl.when(sp > 0)
    def _():
        tail_copy.wait_recv()

    padded[:edge, :] = tail_in[:, :channels]
    padded_docs[:edge, :] = tail_in[:, channels:]
    convolve(0)
    hand_out(0)

    for i in range(DEPTH - 1):
        meta_arrival(i).wait_recv()
        choose(levels[i])

    pair = lax.div(tp, 2) * 2
    odd = tp - pair
    givers = [tp, pair + 1 - odd]
    for q in range(1, tp_count // 2):
        base = lax.rem(pair + 2 * q, tp_count)
        givers += [base + odd, base + 1 - odd]

    for load in loads[7:10]:
        load.wait()
    squares = jnp.zeros((rows, 1), jnp.float32)
    for n, giver in enumerate(givers):
        if n > 0:
            conv_copy(0, giver).wait_recv()
        lines = pl.ds(pl.multiple_of(giver * channels, channels), channels)
        block = conv_in.at[giver][...]
        for c in range(pieces):
            at = slice(c * step, (c + 1) * step)
            mix = jnp.dot(block, proj_w[lines, at], preferred_element_type=jnp.float32)
            if n > 0:
                mix = carried_ref[:, at] + mix
            if n == tp_count - 1:
                mix = residual_ref[:, at].astype(jnp.float32) + mix.astype(jnp.bfloat16).astype(jnp.float32)
                squares = squares + jnp.sum(mix * mix, axis=1, keepdims=True)
            carried_ref[:, at] = mix
    scale = lax.rsqrt(squares / width + 1e-06)

    def x_copy(k, s, c, level):
        return pltpu.make_async_remote_copy(
            src_ref=x_all.at[s, c], dst_ref=x_all.at[s, c], send_sem=x_send.at[k, s, c], recv_sem=x_recv.at[s, c],
            device_id=along(level), device_id_type=MESH,
        )

    def part_copy(s, c, slot, level):
        return pltpu.make_async_remote_copy(
            src_ref=part_out.at[s, c], dst_ref=part_in.at[slot, c],
            send_sem=part_send.at[s, c], recv_sem=part_recv.at[slot, c],
            device_id=along(level), device_id_type=MESH,
        )

    def exchange(origin, target, send, recv, s, c, n):
        return pltpu.make_async_remote_copy(
            src_ref=origin.at[s, c, peers[n]], dst_ref=target.at[s, c, mine],
            send_sem=send.at[s, c], recv_sem=recv.at[s, c],
            device_id=homes[n], device_id_type=MESH,
        )

    def everyone(origin, target, send, recv, s, c):
        return pltpu.make_async_remote_copy(
            src_ref=origin.at[s, c, pl.ds(0, group - 1)], dst_ref=target.at[s, c, pl.ds(0, group - 1)],
            send_sem=send.at[s, c], recv_sem=recv.at[s, c],
            device_id=homes[0], device_id_type=MESH,
        )

    go = (slots, arrived, go_send, go_recv)
    ret = (served, back, ret_send, ret_recv)

    def send_all(way, s, c):
        for n in range(group - 1):
            exchange(*way, s, c, n).start()
        way[1].at[s, c, mine][...] = way[0].at[s, c, mine][...]

    def dispatch(s, c, level=None, own=False):
        if not own:
            x_copy(0, s, c, z).wait_recv()
        if level is not None:
            x_copy(0, s, c, level).start()
        picked = jnp.dot(place.at[s][...], x_all.at[s, c][...], preferred_element_type=jnp.float32)
        slots.at[s, c][...] = picked.astype(jnp.bfloat16).reshape(group, cap, step)
        send_all(go, s, c)

    tile = 256

    def serve(s):
        sums[...] = jnp.zeros(sums.shape, jnp.float32)

        @pl.loop(0, pieces)
        def _(c):
            everyone(*go, s, c).wait_recv()
            block = arrived.at[s, c][...].reshape(slot_count, step)
            lines = pl.ds(pl.multiple_of(c * step, step), step)
            for w, weight in enumerate((gate_w, up_w)):
                for f in range(ff // tile):
                    at = slice(f * tile, (f + 1) * tile)
                    to = slice(w * ff + f * tile, w * ff + (f + 1) * tile)
                    sums[:, to] += jnp.dot(block, weight[lines, at], preferred_element_type=jnp.float32)

        gate_value = sums[:, :ff]
        silu = gate_value * (1.0 / (1.0 + jnp.exp(-gate_value)))
        hidden[...] = (silu * sums[:, ff:]).astype(jnp.bfloat16)

        @pl.loop(0, pieces)
        def _(c):
            for f in range(step // tile):
                at = pl.ds(pl.multiple_of(c * step + f * tile, tile), tile)
                value = jnp.dot(hidden[...], down_w[:, at], preferred_element_type=jnp.float32)
                value = value.astype(jnp.bfloat16).reshape(group, cap, tile)
                served.at[s, c][:, :, f * tile : (f + 1) * tile] = value
            send_all(ret, s, c)

    def weighted(s, c):
        everyone(*ret, s, c).wait_recv()
        got = back.at[s, c][...].reshape(slot_count, step)
        return jnp.dot(high.at[s][...], got, preferred_element_type=jnp.float32) + jnp.dot(
            low.at[s][...], got, preferred_element_type=jnp.float32
        )

    def combine_own(c):
        carried_ref[:, c * step : (c + 1) * step] += weighted(z, c)

    def combine(j, c, slot):
        part_out.at[order[j], c][...] = weighted(order[j], c).astype(jnp.bfloat16)
        part_copy(order[j], c, slot, inner_z).start()

    def hold(j, c):
        held[j, c] = weighted(order[j], c)

    def relay(j, c, slot, level):
        part_copy(order[j], c, order[j], level).wait_recv()
        total = held[j, c] + part_in.at[order[j], c][...].astype(jnp.float32)
        part_out.at[order[j], c][...] = total.astype(jnp.bfloat16)
        part_copy(order[j], c, slot, level).start()

    def finish(c, arrivals):
        total = carried_ref[:, c * step : (c + 1) * step]
        for slot in arrivals:
            part_copy(z, c, slot, inner_z).wait_recv()
            total = total + part_in.at[slot, c][...].astype(jnp.float32)
        out_ref[:, c * step : (c + 1) * step] = total.astype(jnp.bfloat16)

    def slot_from(s, above):
        return s + (DEPTH - s) * above

    x_middle = (inner_z, outer_z, outer_z)
    every = range(pieces)

    for c in every:
        at = slice(c * step, (c + 1) * step)
        x_all.at[z, c][...] = (carried_ref[:, at] * scale * gain_ref[:, at]).astype(jnp.bfloat16)
        x_copy(1, z, c, inner_z).start()
        if c == 0:
            @pl.when(inward > 0)
            def _():
                x_copy(0, z, 0, outer_z).start()
    for c in every:
        dispatch(z, c, own=True)
    for load in loads[10:13]:
        load.wait()
    serve(z)

    @pl.when(is_end)
    def _():
        dispatch(order[0], 0)
        for c in every:
            combine_own(c)
        for c in range(1, pieces):
            dispatch(order[0], c)

    @pl.when(inward > 0)
    def _():
        for c in every:
            dispatch(order[0], c, x_middle[0])
            dispatch(order[1], c, x_middle[1])
        dispatch(order[2], 0, x_middle[2])

    serve(order[0])

    def overlap(j):
        for c in range(pieces - 1):
            dispatch(order[j + 1], c)
        for c in range(pieces - 1):
            combine(j, c, order[j])
        dispatch(order[j + 1], pieces - 1)
        combine(j, pieces - 1, order[j])

    @pl.when(is_end)
    def _():
        overlap(0)

    @pl.when(inward > 0)
    def _():
        dispatch(order[2], 1, x_middle[2])

    serve(order[1])

    @pl.when(is_end)
    def _():
        overlap(1)

    @pl.when(inward > 0)
    def _():
        dispatch(order[2], 2, x_middle[2])
        for c in every:
            combine_own(c)
        for c in every:
            hold(0, c)
        for c in range(3, pieces):
            dispatch(order[2], c, x_middle[2])
        for c in range(1, pieces):
            x_copy(0, z, c, outer_z).start()
        for c in every:
            hold(1, c)

    serve(order[2])

    @pl.when(is_end)
    def _():
        for c in every:
            combine(2, c, slot_from(order[2], 1 - low_half))
        for c in every:
            finish(c, (slot_from(z, low_half),))
        for c in every:
            x_copy(1, z, c, inner_z).wait_send()

    @pl.when(inward > 0)
    def _():
        to_middle = slot_from(order[1], 1 - low_half)
        to_end = slot_from(order[0], low_half)
        for c in range(2):
            relay(1, c, to_middle, inner_z)
        for c in every:
            hold(2, c)
        for c in range(2, pieces):
            relay(1, c, to_middle, inner_z)
        for c in every:
            relay(2, c, order[2], inner_z)
            relay(0, c, to_end, outer_z)
        for c in every:
            finish(c, (z, DEPTH))
        for c in every:
            for k, level in enumerate((outer_z, inner_z)):
                x_copy(k, z, c, level).wait_send()
            for j in range(DEPTH - 1):
                x_copy(0, order[j], c, x_middle[j]).wait_send()

    @pl.when(sp < sp_count - 1)
    def _():
        tail_copy.wait_send()

    for b in range(tp_count):
        @pl.when(tp != b)
        def _():
            conv_copy(b, tp).wait_send()

    for i in range(DEPTH - 1):
        meta_copy(i).wait_send()

    @pl.loop(0, DEPTH)
    def _(s):
        @pl.loop(0, pieces)
        def _(c):
            everyone(*go, s, c).wait_send()
            everyone(*ret, s, c).wait_send()

            @pl.when(s != z)
            def _():
                part_copy(s, c, s, inner_z).wait_send()


def run_layer(front, routing, gate_proj, up_proj, down_proj, out_proj, cap, pieces=4):
    sp_count, tp_count = lax.axis_size("sp"), lax.axis_size("tp")
    length, channels = front[0].shape
    lanes = front[4].shape[1]
    rows, width = front[5].shape
    edge = 8
    ff = gate_proj.shape[2]
    group = sp_count // DEPTH * tp_count
    step = width // pieces
    slot_count = group * cap
    slot_shape = (DEPTH, pieces, group, cap, step)
    f32, bf16 = jnp.float32, jnp.bfloat16
    dma = pltpu.SemaphoreType.DMA
    vmem = pltpu.VMEM
    hbm = pl.BlockSpec(memory_space=pl.ANY)
    arrays = (*front, *routing)
    return pl.pallas_call(
        functools.partial(layer_kernel, sp_count, tp_count, cap, pieces),
        out_shape=jax.ShapeDtypeStruct((rows, width), bf16),
        in_specs=[hbm] * (len(arrays) + 4),
        out_specs=pl.BlockSpec(memory_space=pltpu.VMEM),
        scratch_shapes=[vmem(a.shape, a.dtype) for a in arrays]
        + [
            vmem((width, ff), bf16),
            vmem((width, ff), bf16),
            vmem((ff, width), bf16),
            vmem(out_proj.shape, bf16),
            vmem((edge + length, channels), f32),
            vmem((edge + length, lanes), f32),
            vmem((edge, channels + lanes), f32),
            vmem((edge, channels + lanes), f32),
            vmem((tp_count, rows, channels), bf16),
            vmem((tp_count, rows, channels), bf16),
            vmem((rows, width), f32),
            vmem((DEPTH, 8, rows), f32),
            vmem((DEPTH, slot_count, rows), bf16),
            vmem((slot_count, rows), f32),
            vmem((DEPTH, rows, slot_count), bf16),
            vmem((DEPTH, rows, slot_count), bf16),
            vmem((DEPTH, pieces, rows, step), bf16),
            vmem(slot_shape, bf16),
            vmem(slot_shape, bf16),
            vmem(slot_shape, bf16),
            vmem(slot_shape, bf16),
            vmem((slot_count, ff), bf16),
            vmem((slot_count, 2 * ff), f32),
            vmem((DEPTH - 1, pieces, rows, step), f32),
            vmem((DEPTH, pieces, rows, step), bf16),
            vmem((DEPTH + 1, pieces, rows, step), bf16),
            dma((len(arrays) + 4,)),
            dma((2,)),
            dma((tp_count,)),
            dma((tp_count,)),
            dma((DEPTH - 1,)),
            dma((DEPTH,)),
            dma((2, DEPTH, pieces)),
            dma((DEPTH, pieces)),
            dma((DEPTH, pieces)),
            dma((DEPTH, pieces)),
            dma((DEPTH, pieces)),
            dma((DEPTH, pieces)),
            dma((DEPTH, pieces)),
            dma((DEPTH + 1, pieces)),
        ],
        compiler_params=pltpu.CompilerParams(
            collective_id=0, has_side_effects=True, vmem_limit_bytes=56 * 1024 * 1024
        ),
    )(*arrays, gate_proj, up_proj, down_proj, out_proj)


def from_behind(block, axis, distance):
    devices = range(lax.axis_size(axis))
    route = [(i - distance, i) for i in devices if i - distance in devices]
    return lax.ppermute(block, axis, route)


def expert_rows(arrived, gate_weight, up_weight, down_weight):
    gate_value = jnp.dot(arrived, gate_weight, preferred_element_type=jnp.float32)
    up_value = jnp.dot(arrived, up_weight, preferred_element_type=jnp.float32)
    hidden = (jax.nn.silu(gate_value) * up_value).astype(jnp.bfloat16)
    return jnp.dot(hidden, down_weight, preferred_element_type=jnp.float32).astype(jnp.bfloat16)


def on_device(
    conv_input,
    gate_inner,
    gate_outer,
    conv_taps,
    doc_ids,
    residual_in,
    out_proj,
    norm_gain,
    expert_ids,
    expert_weights,
    gate_proj,
    up_proj,
    down_proj,
):
    sp_count, tp_count = lax.axis_size("sp"), lax.axis_size("tp")
    capacity = 2 * residual_in.shape[0] * expert_ids.shape[1] // (sp_count * tp_count)
    if capacity % 16 == 0 and sp_count % DEPTH == 0 and tp_count % 2 == 0:
        docs = doc_ids.reshape(-1, 128)
        front = (conv_input, gate_inner, gate_outer, conv_taps, docs, residual_in, norm_gain[None, :])
        routing = (expert_ids.T, expert_weights.T)
        return run_layer(front, routing, gate_proj, up_proj, down_proj, out_proj, capacity)
    inner_prod = conv_input.astype(jnp.float32) * gate_inner.astype(jnp.float32)
    earlier, earlier_docs = from_behind((inner_prod[-2:], doc_ids[-2:]), "sp", 1)
    padded = jnp.concatenate([earlier, inner_prod], axis=0)
    padded_docs = jnp.concatenate([earlier_docs, doc_ids], axis=0)
    length = inner_prod.shape[0]
    tap_values = conv_taps.astype(jnp.float32)
    one_back = jnp.where(
        (padded_docs[1 : length + 1] == doc_ids)[:, None], padded[1 : length + 1], 0.0
    )
    two_back = jnp.where((padded_docs[:length] == doc_ids)[:, None], padded[:length], 0.0)
    mixed_rows = tap_values[2] * inner_prod + tap_values[1] * one_back + tap_values[0] * two_back
    conv_out = (gate_outer.astype(jnp.float32) * mixed_rows).astype(jnp.bfloat16)
    row_count = residual_in.shape[0]
    regrouped = lax.all_to_all(conv_out, "tp", split_axis=0, concat_axis=1, tiled=True)
    mix = jnp.dot(regrouped, out_proj, preferred_element_type=jnp.float32).astype(jnp.bfloat16)
    carried = residual_in.astype(jnp.float32) + mix.astype(jnp.float32)
    normed = (
        carried * lax.rsqrt(jnp.mean(carried * carried, axis=1, keepdims=True) + 1e-06) * norm_gain
    ).astype(jnp.bfloat16)
    model_width = normed.shape[1]
    choose = expert_ids.shape[1]
    experts_total = sp_count * tp_count
    flat_ids = expert_ids.reshape(-1)
    onehot = (flat_ids[:, None] == jnp.arange(experts_total, dtype=jnp.int32)[None, :]).astype(
        jnp.int32
    )
    slot_rank = jnp.sum((jnp.cumsum(onehot, axis=0) - 1) * onehot, axis=1)
    target = flat_ids * capacity + slot_rank
    sources = jnp.repeat(normed, choose, axis=0)
    outgoing = (
        jnp.zeros((experts_total * capacity, model_width), jnp.bfloat16).at[target].set(sources)
    )
    gate_weight = gate_proj[0]
    up_weight = up_proj[0]
    down_weight = down_proj[0]
    arrived = lax.all_to_all(
        outgoing.reshape(experts_total, capacity, model_width),
        ("sp", "tp"),
        split_axis=0,
        concat_axis=0,
        tiled=True,
    )
    item_count = arrived.shape[1]
    flat_rows = arrived.reshape(-1, model_width)
    result = expert_rows(flat_rows, gate_weight, up_weight, down_weight)
    result = result.reshape(experts_total, item_count, model_width)
    returned = lax.all_to_all(result, ("sp", "tp"), split_axis=0, concat_axis=0, tiled=True)
    picked = (
        returned.reshape(-1, model_width)[target]
        .reshape(row_count, choose, model_width)
        .astype(jnp.float32)
    )
    combined = carried + jnp.sum(expert_weights[:, :, None] * picked, axis=1)
    return combined.astype(jnp.bfloat16)


def solution(mesh):
    in_specs = (
        P("sp", "tp"),
        P("sp", "tp"),
        P("sp", "tp"),
        P(None, "tp"),
        P("sp"),
        P(("sp", "tp"), None),
        P(),
        P(),
        P(("sp", "tp"), None),
        P(("sp", "tp"), None),
        P(("sp", "tp"), None, None),
        P(("sp", "tp"), None, None),
        P(("sp", "tp"), None, None),
    )
    out_specs = P(("sp", "tp"), None)
    return jax.shard_map(
        on_device, mesh=mesh, in_specs=in_specs, out_specs=out_specs, check_vma=False
    )
```

time: 108 us -> 98.9 us (0.916)
  local copies, waits for them, and re-layouts: 7.63 us -> 1.88 us
  other arithmetic: 2.81 us -> 0 us
    unnamed x14 -> x1, local copies, waits for them, and re-layouts: 6.85 us -> 1.88 us
where the time goes in v1:
time: 98.9 us; the launch traced here: 98.7 us
  Pallas kernels  96.9 us (98%)
  local copies, waits for them, and re-layouts  1.88 us (2%)
    pallas_call x1, Pallas kernels, run_layer(): pl.pallas_call(functools.partial(layer_kernel, sp_count, tp_count, cap, p...  96.9 us

profile of v1, /device:TPU:0, one launch (start us, length us, event | category | flops | bytes accessed | tf_op | source)
XLA Modules:
  0.0 98.7 jit_solution(4224508879841263161)
XLA Ops:
  0.0 96.9 %shard_map.127 = bf16[128,2048]{1,0:T(8,128)(2,1)} custom-call(bf16[512,256]{1,0:T(8,128)(2,1)} %conv_hbm.1, bf16[512,256]{1,0:T(8,128)(2,1)} %inner_hbm.1, bf16[512,256]{1,0:T(8,128)(2,1)} %outer_hbm.1, bf16[3,256]{1,0:T(4,128)(2,1)} %taps_hbm.1, s32[4,128]{1,0:T(4,128)} %bitcast.5, bf16[128,2048]{1,0:T(8,128)(2,1)} %residual_hbm.1, f32[1,2048]{1,0:T(1,128)} %bitcast.4, ...), custom_call_target="tpu_custom_call" | custom-call | tf_op jit(solution)/shard_map/pallas_call | solution.py:496
  96.9 1.9 %copy.15 = bf16[128,2048]{1,0:T(8,128)(2,1)} copy(bf16[128,2048]{1,0:T(8,128)(2,1)} %shard_map.127) | data formatting | bytes 1048576

commit v2 on v1

--- a/solution.py
+++ b/solution.py
@@ -18,9 +18,9 @@
     out_ref,
     conv_ref, inner_ref, outer_ref, taps_ref, docs_ref, residual_ref, gain_ref, ids_ref, scores_ref,
     gate_w, up_w, down_w, proj_w,
-    padded, padded_docs, tail, tail_in, conv_out, conv_in, carried_ref,
+    padded, padded_docs, tail, tail_in, fix, fix_in, conv_out, conv_in, carried_ref,
     metas, place, wide, high, low, x_all, slots, arrived, served, back, hidden, sums, held, part_out, part_in,
-    load_sem, tail_sem, conv_send, conv_recv, meta_send, meta_recv, x_send, x_recv,
+    load_sem, tail_send, tail_recv, fix_send, fix_recv, conv_send, conv_recv, meta_send, meta_recv, x_send, x_recv,
     go_send, go_recv, ret_send, ret_recv, part_send, part_recv,
 ):
     sp = lax.axis_index("sp")
@@ -46,11 +46,8 @@
     def source(end, middle):
         return flip(end * (1 - inward) + middle * inward)
 
-    order = (source(2, 0), source(3, 2), source(1, 3))
+    order = (source(2, 2), source(3, 0), source(1, 3))
     outer_z, inner_z = flip(inward - 1), flip(inward + 1)
-
-    def peer(i):
-        return lax.rem(mine + i, group)
 
     def where(member):
         return (z * span + lax.div(member, tp_count), lax.rem(member, tp_count))
@@ -58,7 +55,22 @@
     def along(level):
         return (level * span + y, tp)
 
-    peers = [peer(group - 1 - i) for i in range(group - 1)]
+    pair = lax.div(tp, 2) * 2
+    odd = tp - pair
+    givers = [tp, pair + 1 - odd]
+    for q in range(1, tp_count // 2):
+        base = lax.rem(pair + 2 * q, tp_count)
+        givers += [base + odd, base + 1 - odd]
+
+    peers = []
+    for i in range(span - 1, 0, -1):
+        side = lax.rem(y + i, span) * tp_count
+        peers += [side + t for t in givers[2:]]
+    near = [lax.rem(y + i, span) * tp_count + t for i in range(1, span) for t in givers[:2]]
+    here = [y * tp_count + t for t in givers[2:]]
+    for i in range(max(len(near), len(here))):
+        peers += near[i : i + 1] + here[i : i + 1]
+    peers.append(y * tp_count + givers[1])
     homes = [where(other) for other in peers]
 
     pairs = (
@@ -79,13 +91,10 @@
     for level in levels:
         pl.semaphore_signal(barrier, inc=1, device_id=along(level), device_id_type=MESH)
 
-    @pl.when(sp < sp_count - 1)
-    def _():
-        pl.semaphore_signal(barrier, inc=1, device_id=(sp + 1, tp), device_id_type=MESH)
-
-    @pl.when(sp > 0)
-    def _():
-        pl.semaphore_signal(barrier, inc=1, device_id=(sp - 1, tp), device_id_type=MESH)
+    for t in range(tp_count):
+        @pl.when((tp == 0) & (sp > 0))
+        def _():
+            pl.semaphore_signal(barrier, inc=1, device_id=(sp - 1, t), device_id_type=MESH)
 
     length, channels = conv_ref.shape
     lanes = tail.shape[1] - channels
@@ -97,6 +106,8 @@
     for j in range(length // lanes):
         at = slice(edge + j * lanes, edge + (j + 1) * lanes)
         padded_docs[at, :] = jnp.broadcast_to(docs[j : j + 1, :], (lanes, lanes)).T
+    padded[:edge, :] = jnp.zeros((edge, channels), jnp.float32)
+    padded_docs[:edge, :] = jnp.full((edge, lanes), -1.0, jnp.float32)
     tail[:, :channels] = padded[length:, :]
     tail[:, channels:] = padded_docs[length:, :]
     for load in loads[3:5]:
@@ -133,7 +144,17 @@
         def _():
             conv_in[b] = conv_out[b]
 
-    for b in range(1, tp_count):
+    for k in range(channels // lanes):
+        at = slice(k * lanes, (k + 1) * lanes)
+        same_one = padded_docs[edge - 1 : 2 * edge - 1, :] == padded_docs[edge : 2 * edge, :]
+        one_back = jnp.where(same_one, padded[edge - 1 : 2 * edge - 1, at], 0.0)
+        mixed = taps[2:3, at] * padded[edge : 2 * edge, at] + taps[1:2, at] * one_back
+        fix[0:2, at] = mixed[0:2]
+    fix[2:4, :] = outer_ref[0:2, :].astype(jnp.float32)
+    fix[4:6, :] = taps[0:2]
+    fix[6:8, :] = jnp.zeros((2, channels), jnp.float32)
+
+    for b in range(tp_count):
         convolve(b)
     for load in loads[5:7]:
         load.wait()
@@ -141,21 +162,63 @@
     metas.at[z][2:4, :] = scores_ref[...]
     metas.at[z][4:, :] = jnp.zeros((4, rows), jnp.float32)
 
-    behind = lax.div(sp + sp_count - 1, sp_count)
     ahead = lax.div(2 * sp_count - 2 - sp, sp_count)
-    pl.semaphore_wait(barrier, group - 1 + DEPTH - 1 + behind + ahead)
-
-    tail_copy = pltpu.make_async_remote_copy(
-        src_ref=tail, dst_ref=tail_in, send_sem=tail_sem.at[0], recv_sem=tail_sem.at[1],
-        device_id=(lax.rem(sp + 1, sp_count), tp), device_id_type=MESH,
-    )
-
-    @pl.when(sp < sp_count - 1)
-    def _():
-        tail_copy.start()
+    pl.semaphore_wait(barrier, group - 1 + DEPTH - 1 + ahead)
+
+    def tail_copy(t, level):
+        return pltpu.make_async_remote_copy(
+            src_ref=tail, dst_ref=tail_in.at[t], send_sem=tail_send.at[0], recv_sem=tail_recv.at[t],
+            device_id=(level, 0), device_id_type=MESH,
+        )
+
+    def fix_copy(t):
+        return pltpu.make_async_remote_copy(
+            src_ref=fix, dst_ref=fix_in.at[t], send_sem=fix_send.at[0], recv_sem=fix_recv.at[t],
+            device_id=(sp, 0), device_id_type=MESH,
+        )
+
+    has_next = sp < sp_count - 1
+    completes = (tp == 0) & (sp > 0)
+    helps = (tp > 0) & (sp > 0)
+
+    @pl.when(has_next)
+    def _():
+        tail_copy(tp, lax.rem(sp + 1, sp_count)).start()
 
     for b in range(1, tp_count):
         hand_out(b)
+
+    @pl.when(helps)
+    def _():
+        fix_copy(tp).start()
+
+    hand_out(0)
+
+    @pl.when(completes)
+    def _():
+        fix_in[0] = fix[...]
+
+    def complete(n):
+        tail_copy(n, sp).wait_recv()
+        if n > 0:
+            fix_copy(n).wait_recv()
+        line = lax.broadcasted_iota(jnp.int32, (16, lanes), 0)
+        first_doc, second_doc = padded_docs[edge : edge + 1, :], padded_docs[edge + 1 : edge + 2, :]
+        last_doc = tail_in[n, edge - 1 : edge, channels:]
+        far_doc = tail_in[n, edge - 2 : edge - 1, channels:]
+        for k in range(channels // lanes):
+            at = slice(k * lanes, (k + 1) * lanes)
+            last, far = tail_in[n, edge - 1 : edge, at], tail_in[n, edge - 2 : edge - 1, at]
+            oldest, older = fix_in[n, 4:5, at], fix_in[n, 5:6, at]
+            mixed = fix_in[n, 0:1, at] + older * jnp.where(last_doc == first_doc, last, 0.0)
+            mixed = mixed + oldest * jnp.where(far_doc == first_doc, far, 0.0)
+            row_zero = fix_in[n, 2:3, at] * mixed
+            mixed = fix_in[n, 1:2, at] + oldest * jnp.where(last_doc == second_doc, last, 0.0)
+            row_one = fix_in[n, 3:4, at] * mixed
+            was = conv_in[n, 0:16, at].astype(jnp.float32)
+            now = jnp.where(line == 0, row_zero, jnp.where(line == 1, row_one, was))
+            conv_in[n, 0:16, at] = now.astype(jnp.bfloat16)
+
 
     def meta_copy(i):
         return pltpu.make_async_remote_copy(
@@ -201,37 +264,17 @@
 
     choose(z)
 
-    @pl.when(sp == 0)
-    def _():
-        tail_in[:, :channels] = jnp.zeros((edge, channels), jnp.float32)
-        tail_in[:, channels:] = jnp.full((edge, lanes), -1.0, jnp.float32)
-
-    @pl.when(sp > 0)
-    def _():
-        tail_copy.wait_recv()
-
-    padded[:edge, :] = tail_in[:, :channels]
-    padded_docs[:edge, :] = tail_in[:, channels:]
-    convolve(0)
-    hand_out(0)
-
-    for i in range(DEPTH - 1):
-        meta_arrival(i).wait_recv()
-        choose(levels[i])
-
-    pair = lax.div(tp, 2) * 2
-    odd = tp - pair
-    givers = [tp, pair + 1 - odd]
-    for q in range(1, tp_count // 2):
-        base = lax.rem(pair + 2 * q, tp_count)
-        givers += [base + odd, base + 1 - odd]
-
     for load in loads[7:10]:
         load.wait()
     squares = jnp.zeros((rows, 1), jnp.float32)
     for n, giver in enumerate(givers):
         if n > 0:
             conv_copy(0, giver).wait_recv()
+
+        @pl.when(completes)
+        def _():
+            complete(n)
+
         lines = pl.ds(pl.multiple_of(giver * channels, channels), channels)
         block = conv_in.at[giver][...]
         for c in range(pieces):
@@ -291,24 +334,24 @@
 
     tile = 256
 
-    def serve(s):
+    def serve_up(s, between=None):
         sums[...] = jnp.zeros(sums.shape, jnp.float32)
-
-        @pl.loop(0, pieces)
-        def _(c):
+        for c in every:
             everyone(*go, s, c).wait_recv()
             block = arrived.at[s, c][...].reshape(slot_count, step)
-            lines = pl.ds(pl.multiple_of(c * step, step), step)
+            lines = slice(c * step, (c + 1) * step)
             for w, weight in enumerate((gate_w, up_w)):
                 for f in range(ff // tile):
                     at = slice(f * tile, (f + 1) * tile)
                     to = slice(w * ff + f * tile, w * ff + (f + 1) * tile)
                     sums[:, to] += jnp.dot(block, weight[lines, at], preferred_element_type=jnp.float32)
-
+            if between is not None:
+                between(c)
         gate_value = sums[:, :ff]
         silu = gate_value * (1.0 / (1.0 + jnp.exp(-gate_value)))
         hidden[...] = (silu * sums[:, ff:]).astype(jnp.bfloat16)
 
+    def serve_down(s, sends=None):
         @pl.loop(0, pieces)
         def _(c):
             for f in range(step // tile):
@@ -316,7 +359,10 @@
                 value = jnp.dot(hidden[...], down_w[:, at], preferred_element_type=jnp.float32)
                 value = value.astype(jnp.bfloat16).reshape(group, cap, tile)
                 served.at[s, c][:, :, f * tile : (f + 1) * tile] = value
-            send_all(ret, s, c)
+            if sends is True:
+                send_all(ret, s, c)
+            elif sends is not None:
+                pl.when(sends)(lambda: send_all(ret, s, c))
 
     def weighted(s, c):
         everyone(*ret, s, c).wait_recv()
@@ -351,100 +397,162 @@
     def slot_from(s, above):
         return s + (DEPTH - s) * above
 
-    x_middle = (inner_z, outer_z, outer_z)
+    x_middle = (outer_z, inner_z, outer_z)
+    lead = pieces // 2
     every = range(pieces)
 
     for c in every:
         at = slice(c * step, (c + 1) * step)
         x_all.at[z, c][...] = (carried_ref[:, at] * scale * gain_ref[:, at]).astype(jnp.bfloat16)
         x_copy(1, z, c, inner_z).start()
-        if c == 0:
+        if c < lead:
             @pl.when(inward > 0)
             def _():
-                x_copy(0, z, 0, outer_z).start()
+                x_copy(0, z, c, outer_z).start()
     for c in every:
         dispatch(z, c, own=True)
+    for i in range(DEPTH - 1):
+        meta_arrival(i).wait_recv()
+        choose(levels[i])
     for load in loads[10:13]:
         load.wait()
-    serve(z)
-
-    @pl.when(is_end)
-    def _():
-        dispatch(order[0], 0)
-        for c in every:
-            combine_own(c)
-        for c in range(1, pieces):
+
+    def at_end(todo):
+        pl.when(is_end)(todo)
+
+    def in_middle(todo):
+        pl.when(inward > 0)(todo)
+
+    def first_hook(c):
+        if c == 1:
+            @in_middle
+            def _():
+                dispatch(order[0], 0, x_middle[0])
+                dispatch(order[1], 0, x_middle[1])
+        if c == 2:
+            @at_end
+            def _():
+                dispatch(order[2], 0)
+
+    serve_up(z, first_hook)
+
+    @in_middle
+    def _():
+        dispatch(order[0], 1, x_middle[0])
+        dispatch(order[1], 1, x_middle[1])
+
+    @at_end
+    def _():
+        for c in range(1, lead):
+            dispatch(order[2], c)
+
+    serve_down(z)
+
+    @at_end
+    def _():
+        send_all(ret, z, 0)
+        send_all(ret, z, 1)
+        for c in every:
             dispatch(order[0], c)
-
-    @pl.when(inward > 0)
-    def _():
-        for c in every:
+            if c + 2 < pieces:
+                send_all(ret, z, c + 2)
+
+    @in_middle
+    def _():
+        for c in range(2, pieces):
             dispatch(order[0], c, x_middle[0])
             dispatch(order[1], c, x_middle[1])
-        dispatch(order[2], 0, x_middle[2])
-
-    serve(order[0])
-
-    def overlap(j):
-        for c in range(pieces - 1):
-            dispatch(order[j + 1], c)
-        for c in range(pieces - 1):
-            combine(j, c, order[j])
-        dispatch(order[j + 1], pieces - 1)
-        combine(j, pieces - 1, order[j])
-
-    @pl.when(is_end)
-    def _():
-        overlap(0)
-
-    @pl.when(inward > 0)
+
+    def second_hook(c):
+        if c == 2:
+            @in_middle
+            def _():
+                dispatch(order[2], 0, x_middle[2])
+
+    serve_up(order[0], second_hook)
+
+    @at_end
+    def _():
+        dispatch(order[1], 0)
+
+    serve_down(order[0], True)
+
+    @at_end
+    def _():
+        dispatch(order[1], 1)
+        for c in every:
+            combine_own(c)
+        combine(0, 0, order[0])
+        dispatch(order[1], 2)
+        combine(0, 1, order[0])
+        combine(0, 2, order[0])
+        dispatch(order[1], 3)
+        combine(0, 3, order[0])
+
+    @in_middle
     def _():
         dispatch(order[2], 1, x_middle[2])
 
-    serve(order[1])
-
-    @pl.when(is_end)
-    def _():
-        overlap(1)
-
-    @pl.when(inward > 0)
-    def _():
-        dispatch(order[2], 2, x_middle[2])
+    serve_up(order[1])
+
+    @at_end
+    def _():
+        dispatch(order[2], 2)
+
+    serve_down(order[1], is_end)
+
+    @at_end
+    def _():
+        dispatch(order[2], 3)
+        for c in every:
+            combine(1, c, order[1])
+
+    @in_middle
+    def _():
+        for c in range(2, pieces):
+            dispatch(order[2], c, x_middle[2])
+        for c in range(lead, pieces):
+            x_copy(0, z, c, outer_z).start()
+        for c in every:
+            send_all(ret, order[1], c)
+        for c in every:
+            hold(0, c)
+
+    serve_up(order[2])
+    serve_down(order[2], True)
+
+    @at_end
+    def _():
+        for c in every:
+            combine(2, c, slot_from(order[2], 1 - low_half))
+        for c in every:
+            finish(c, (slot_from(z, low_half),))
+        for c in every:
+            x_copy(1, z, c, inner_z).wait_send()
+
+    @in_middle
+    def _():
+        to_middle = slot_from(order[0], 1 - low_half)
+        to_end = slot_from(order[1], low_half)
+        for c in every:
+            send_all(ret, z, c)
+        relay(0, 0, to_middle, inner_z)
+        for c in every:
+            hold(1, c)
+        relay(0, 1, to_middle, inner_z)
+        relay(0, 2, to_middle, inner_z)
+        hold(2, 0)
+        hold(2, 1)
+        relay(0, 3, to_middle, inner_z)
+        hold(2, 2)
+        hold(2, 3)
+        relay(2, 0, order[2], inner_z)
         for c in every:
             combine_own(c)
-        for c in every:
-            hold(0, c)
-        for c in range(3, pieces):
-            dispatch(order[2], c, x_middle[2])
-        for c in range(1, pieces):
-            x_copy(0, z, c, outer_z).start()
-        for c in every:
-            hold(1, c)
-
-    serve(order[2])
-
-    @pl.when(is_end)
-    def _():
-        for c in every:
-            combine(2, c, slot_from(order[2], 1 - low_half))
-        for c in every:
-            finish(c, (slot_from(z, low_half),))
-        for c in every:
-            x_copy(1, z, c, inner_z).wait_send()
-
-    @pl.when(inward > 0)
-    def _():
-        to_middle = slot_from(order[1], 1 - low_half)
-        to_end = slot_from(order[0], low_half)
-        for c in range(2):
-            relay(1, c, to_middle, inner_z)
-        for c in every:
-            hold(2, c)
-        for c in range(2, pieces):
-            relay(1, c, to_middle, inner_z)
-        for c in every:
-            relay(2, c, order[2], inner_z)
-            relay(0, c, to_end, outer_z)
+        for c in range(1, pieces + 1):
+            if c < pieces:
+                relay(2, c, order[2], inner_z)
+            relay(1, c - 1, to_end, outer_z)
         for c in every:
             finish(c, (z, DEPTH))
         for c in every:
@@ -453,9 +561,13 @@
             for j in range(DEPTH - 1):
                 x_copy(0, order[j], c, x_middle[j]).wait_send()
 
-    @pl.when(sp < sp_count - 1)
-    def _():
-        tail_copy.wait_send()
+    @pl.when(has_next)
+    def _():
+        tail_copy(tp, lax.rem(sp + 1, sp_count)).wait_send()
+
+    @pl.when(helps)
+    def _():
+        fix_copy(tp).wait_send()
 
     for b in range(tp_count):
         @pl.when(tp != b)
@@ -507,7 +619,9 @@
             vmem((edge + length, channels), f32),
             vmem((edge + length, lanes), f32),
             vmem((edge, channels + lanes), f32),
-            vmem((edge, channels + lanes), f32),
+            vmem((tp_count, edge, channels + lanes), f32),
+            vmem((edge, channels), f32),
+            vmem((tp_count, edge, channels), f32),
             vmem((tp_count, rows, channels), bf16),
             vmem((tp_count, rows, channels), bf16),
             vmem((rows, width), f32),
@@ -527,7 +641,10 @@
             vmem((DEPTH, pieces, rows, step), bf16),
             vmem((DEPTH + 1, pieces, rows, step), bf16),
             dma((len(arrays) + 4,)),
-            dma((2,)),
+            dma((1,)),
+            dma((tp_count,)),
+            dma((1,)),
+            dma((tp_count,)),
             dma((tp_count,)),
             dma((tp_count,)),
             dma((DEPTH - 1,)),

time: 98.9 us -> 81.7 us (0.83)
  Pallas kernels: 96.9 us -> 79.7 us
    pallas_call x1, Pallas kernels: 96.9 us -> 79.7 us  [run_layer(): pl.pallas_call(functools.partial(layer_kernel, sp_count, tp_count, cap, p...]
where the time goes in v2:
time: 81.7 us; the launch traced here: 81.6 us
  Pallas kernels  79.7 us (98%)
  local copies, waits for them, and re-layouts  1.88 us (2%)
    pallas_call x1, Pallas kernels, run_layer(): pl.pallas_call(functools.partial(layer_kernel, sp_count, tp_count, cap, p...  79.7 us
    unnamed x1, local copies, waits for them, and re-layouts  1.88 us

profile of v2, /device:TPU:0, one launch (start us, length us, event | category | flops | bytes accessed | tf_op | source)
XLA Modules:
  0.0 81.6 jit_solution(367370566188114621)
XLA Ops:
  0.0 79.7 %shard_map.127 = bf16[128,2048]{1,0:T(8,128)(2,1)} custom-call(bf16[512,256]{1,0:T(8,128)(2,1)} %conv_hbm.1, bf16[512,256]{1,0:T(8,128)(2,1)} %inner_hbm.1, bf16[512,256]{1,0:T(8,128)(2,1)} %outer_hbm.1, bf16[3,256]{1,0:T(4,128)(2,1)} %taps_hbm.1, s32[4,128]{1,0:T(4,128)} %bitcast.5, bf16[128,2048]{1,0:T(8,128)(2,1)} %residual_hbm.1, f32[1,2048]{1,0:T(1,128)} %bitcast.4, ...), custom_call_target="tpu_custom_call" | custom-call | tf_op jit(solution)/shard_map/pallas_call | solution.py:608
  79.7 1.9 %copy.15 = bf16[128,2048]{1,0:T(8,128)(2,1)} copy(bf16[128,2048]{1,0:T(8,128)(2,1)} %shard_map.127) | data formatting | bytes 1048576

commit v3 on v2

--- a/solution.py
+++ b/solution.py
@@ -87,9 +87,11 @@
     barrier = pltpu.get_barrier_semaphore()
     for home in homes:
         pl.semaphore_signal(barrier, inc=1, device_id=home, device_id_type=MESH)
-    levels = [lax.rem(z + i, DEPTH) for i in range(1, DEPTH)]
-    for level in levels:
-        pl.semaphore_signal(barrier, inc=1, device_id=along(level), device_id_type=MESH)
+    pl.semaphore_signal(barrier, inc=1, device_id=along(inner_z), device_id_type=MESH)
+
+    @pl.when(inward > 0)
+    def _():
+        pl.semaphore_signal(barrier, inc=1, device_id=along(outer_z), device_id_type=MESH)
 
     for t in range(tp_count):
         @pl.when((tp == 0) & (sp > 0))
@@ -163,7 +165,7 @@
     metas.at[z][4:, :] = jnp.zeros((4, rows), jnp.float32)
 
     ahead = lax.div(2 * sp_count - 2 - sp, sp_count)
-    pl.semaphore_wait(barrier, group - 1 + DEPTH - 1 + ahead)
+    pl.semaphore_wait(barrier, group + inward + ahead)
 
     def tail_copy(t, level):
         return pltpu.make_async_remote_copy(
@@ -185,14 +187,14 @@
     def _():
         tail_copy(tp, lax.rem(sp + 1, sp_count)).start()
 
+    hand_out(0)
+
+    @pl.when(helps)
+    def _():
+        fix_copy(tp).start()
+
     for b in range(1, tp_count):
         hand_out(b)
-
-    @pl.when(helps)
-    def _():
-        fix_copy(tp).start()
-
-    hand_out(0)
 
     @pl.when(completes)
     def _():
@@ -220,21 +222,17 @@
             conv_in[n, 0:16, at] = now.astype(jnp.bfloat16)
 
 
-    def meta_copy(i):
+    def meta_copy(k, s, level):
         return pltpu.make_async_remote_copy(
-            src_ref=metas.at[z], dst_ref=metas.at[z], send_sem=meta_send.at[i], recv_sem=meta_recv.at[z],
-            device_id=along(levels[i]), device_id_type=MESH,
+            src_ref=metas.at[s], dst_ref=metas.at[s], send_sem=meta_send.at[k], recv_sem=meta_recv.at[s],
+            device_id=along(level), device_id_type=MESH,
         )
 
-    def meta_arrival(i):
-        return pltpu.make_async_remote_copy(
-            src_ref=metas.at[levels[i]], dst_ref=metas.at[levels[i]],
-            send_sem=meta_send.at[i], recv_sem=meta_recv.at[levels[i]],
-            device_id=along(levels[i]), device_id_type=MESH,
-        )
-
-    for i in range(DEPTH - 1):
-        meta_copy(i).start()
+    meta_copy(0, z, inner_z).start()
+
+    @pl.when(inward > 0)
+    def _():
+        meta_copy(1, z, outer_z).start()
 
     first_expert = (z * group).astype(jnp.float32)
     ids = lax.broadcasted_iota(jnp.int32, (group, rows), 0).astype(jnp.float32) + first_expert
@@ -290,28 +288,28 @@
 
     def x_copy(k, s, c, level):
         return pltpu.make_async_remote_copy(
-            src_ref=x_all.at[s, c], dst_ref=x_all.at[s, c], send_sem=x_send.at[k, s, c], recv_sem=x_recv.at[s, c],
+            src_ref=x_all.at[s, c], dst_ref=x_all.at[s, c], send_sem=x_send.at[k], recv_sem=x_recv.at[s, c],
             device_id=along(level), device_id_type=MESH,
         )
 
     def part_copy(s, c, slot, level):
         return pltpu.make_async_remote_copy(
             src_ref=part_out.at[s, c], dst_ref=part_in.at[slot, c],
-            send_sem=part_send.at[s, c], recv_sem=part_recv.at[slot, c],
+            send_sem=part_send.at[0], recv_sem=part_recv.at[slot, c],
             device_id=along(level), device_id_type=MESH,
         )
 
     def exchange(origin, target, send, recv, s, c, n):
         return pltpu.make_async_remote_copy(
             src_ref=origin.at[s, c, peers[n]], dst_ref=target.at[s, c, mine],
-            send_sem=send.at[s, c], recv_sem=recv.at[s, c],
+            send_sem=send.at[0], recv_sem=recv.at[s, c],
             device_id=homes[n], device_id_type=MESH,
         )
 
     def everyone(origin, target, send, recv, s, c):
         return pltpu.make_async_remote_copy(
             src_ref=origin.at[s, c, pl.ds(0, group - 1)], dst_ref=target.at[s, c, pl.ds(0, group - 1)],
-            send_sem=send.at[s, c], recv_sem=recv.at[s, c],
+            send_sem=send.at[0], recv_sem=recv.at[s, c],
             device_id=homes[0], device_id_type=MESH,
         )
 
@@ -351,18 +349,19 @@
         silu = gate_value * (1.0 / (1.0 + jnp.exp(-gate_value)))
         hidden[...] = (silu * sums[:, ff:]).astype(jnp.bfloat16)
 
-    def serve_down(s, sends=None):
-        @pl.loop(0, pieces)
-        def _(c):
+    def serve_down(s, sends=None, between=None):
+        for c in every:
             for f in range(step // tile):
-                at = pl.ds(pl.multiple_of(c * step + f * tile, tile), tile)
+                at = slice(c * step + f * tile, c * step + (f + 1) * tile)
                 value = jnp.dot(hidden[...], down_w[:, at], preferred_element_type=jnp.float32)
                 value = value.astype(jnp.bfloat16).reshape(group, cap, tile)
                 served.at[s, c][:, :, f * tile : (f + 1) * tile] = value
             if sends is True:
                 send_all(ret, s, c)
             elif sends is not None:
-                pl.when(sends)(lambda: send_all(ret, s, c))
+                pl.when(sends)(functools.partial(send_all, ret, s, c))
+            if between is not None:
+                between(c)
 
     def weighted(s, c):
         everyone(*ret, s, c).wait_recv()
@@ -394,12 +393,26 @@
             total = total + part_in.at[slot, c][...].astype(jnp.float32)
         out_ref[:, c * step : (c + 1) * step] = total.astype(jnp.bfloat16)
 
+    def all_sent(ref, sem):
+        pltpu.make_async_remote_copy(
+            src_ref=ref, dst_ref=ref, send_sem=sem, recv_sem=sem, device_id=homes[0], device_id_type=MESH
+        ).wait_send()
+
+    def slots_sent():
+        all_sent(slots.at[:, :, pl.ds(0, group - 1)], go_send.at[0])
+        all_sent(served.at[:, :, pl.ds(0, group - 1)], ret_send.at[0])
+        all_sent(x_all.at[0], x_send.at[1])
+
     def slot_from(s, above):
         return s + (DEPTH - s) * above
 
     x_middle = (outer_z, inner_z, outer_z)
-    lead = pieces // 2
+    lead = max(pieces // 4, 1)
     every = range(pieces)
+
+    def quarter(first, last=None):
+        last = first + 1 if last is None else last
+        return range(first * pieces // 4, last * pieces // 4)
 
     for c in every:
         at = slice(c * step, (c + 1) * step)
@@ -408,12 +421,9 @@
         if c < lead:
             @pl.when(inward > 0)
             def _():
-                x_copy(0, z, c, outer_z).start()
+                x_copy(2, z, c, outer_z).start()
     for c in every:
         dispatch(z, c, own=True)
-    for i in range(DEPTH - 1):
-        meta_arrival(i).wait_recv()
-        choose(levels[i])
     for load in loads[10:13]:
         load.wait()
 
@@ -423,143 +433,153 @@
     def in_middle(todo):
         pl.when(inward > 0)(todo)
 
-    def first_hook(c):
-        if c == 1:
-            @in_middle
-            def _():
-                dispatch(order[0], 0, x_middle[0])
-                dispatch(order[1], 0, x_middle[1])
-        if c == 2:
-            @at_end
-            def _():
-                dispatch(order[2], 0)
-
-    serve_up(z, first_hook)
+    def meet(j, level=None):
+        meta_copy(0, order[j], z).wait_recv()
+        if level is not None:
+            meta_copy(2 + j, order[j], level).start()
+        choose(order[j])
+
+    def arrive(j, *cs):
+        for c in cs:
+            if c == 0:
+                meet(j)
+            dispatch(order[j], c, None)
+
+    def pass_on(j, *cs):
+        for c in cs:
+            if c == 0:
+                meet(j, x_middle[j])
+            dispatch(order[j], c, x_middle[j])
+
+    def spread(*cs):
+        for c in cs:
+            pass_on(0, c)
+            pass_on(1, c)
+
+    def hooks(end, middle):
+        def run(c):
+            if c in end:
+                at_end(end[c])
+            if c in middle:
+                in_middle(middle[c])
+
+        return run
+
+    def then(todo, *args):
+        return functools.partial(todo, *args)
+
+    def start_down():
+        arrive(2, *range(lead))
+        arrive(0, 0)
+
+    in_middle(then(spread, 0))
+    serve_up(
+        z,
+        hooks(
+            {7: start_down},
+            {0: then(spread, 1), 2: then(spread, 2), 4: then(spread, 3), 7: then(spread, 4)},
+        ),
+    )
+    serve_down(z, None, hooks({3: then(arrive, 0, 1)}, {}))
+
+    @at_end
+    def _():
+        for c in range(2, pieces):
+            arrive(0, c)
+            if c < pieces - 2:
+                send_all(ret, z, c - 2)
 
     @in_middle
     def _():
-        dispatch(order[0], 1, x_middle[0])
-        dispatch(order[1], 1, x_middle[1])
+        spread(5, 6, 7)
+
+    serve_up(
+        order[0],
+        hooks(
+            {6: then(arrive, 1, 0)},
+            {3: then(pass_on, 2, 0), 5: then(pass_on, 2, 1), 6: then(pass_on, 2, 2)},
+        ),
+    )
+    def send_back(j, *cs):
+        for c in cs:
+            send_all(ret, order[j], c)
+
+    def both(first, second):
+        def run():
+            first()
+            second()
+
+        return run
+
+    def reply(c):
+        if c < 5:
+            send_back(0, c)
+        else:
+            in_middle(then(send_back, 0, c))
+        hooks(
+            {1: then(arrive, 1, 1), 5: then(arrive, 1, 2)},
+            {1: then(pass_on, 2, 3), 6: then(pass_on, 2, 4)},
+        )(c)
+
+    serve_down(order[0], None, reply)
+
+    def hand_on(j, *cs):
+        for c in cs:
+            combine(j, c, order[j])
 
     @at_end
     def _():
-        for c in range(1, lead):
-            dispatch(order[2], c)
-
-    serve_down(z)
+        for c in range(3, 6):
+            hand_on(0, c - 3)
+            arrive(1, c)
+            send_back(0, c + 2)
+        hand_on(0, 3)
+        arrive(1, 6)
+        hand_on(0, 4)
+        arrive(1, 7)
+        hand_on(0, 5)
+
+    serve_up(
+        order[1],
+        hooks(
+            {3: then(hand_on, 0, 6), 5: then(hand_on, 0, 7)},
+            {1: then(pass_on, 2, 5), 7: then(pass_on, 2, 6)},
+        ),
+    )
+
+    serve_down(
+        order[1],
+        None,
+        hooks(
+            {
+                0: then(send_back, 1, 0),
+                1: both(then(send_back, 1, 1), then(arrive, 2, 2)),
+                2: then(send_back, 1, 2),
+                3: both(then(send_back, 1, 3), then(arrive, 2, 3)),
+                5: then(arrive, 2, 4),
+                7: then(arrive, 2, 5),
+            },
+            {3: then(pass_on, 2, 7)},
+        ),
+    )
 
     @at_end
     def _():
-        send_all(ret, z, 0)
-        send_all(ret, z, 1)
-        for c in every:
-            dispatch(order[0], c)
-            if c + 2 < pieces:
-                send_all(ret, z, c + 2)
+        arrive(2, 6)
+        send_back(1, 4, 5)
+        hand_on(1, 0)
+        arrive(2, 7)
+        send_back(1, 6, 7)
+        hand_on(1, 1, 2, 3)
 
     @in_middle
     def _():
-        for c in range(2, pieces):
-            dispatch(order[0], c, x_middle[0])
-            dispatch(order[1], c, x_middle[1])
-
-    def second_hook(c):
-        if c == 2:
-            @in_middle
-            def _():
-                dispatch(order[2], 0, x_middle[2])
-
-    serve_up(order[0], second_hook)
-
-    @at_end
-    def _():
-        dispatch(order[1], 0)
-
-    serve_down(order[0], True)
-
-    @at_end
-    def _():
-        dispatch(order[1], 1)
-        for c in every:
-            combine_own(c)
-        combine(0, 0, order[0])
-        dispatch(order[1], 2)
-        combine(0, 1, order[0])
-        combine(0, 2, order[0])
-        dispatch(order[1], 3)
-        combine(0, 3, order[0])
-
-    @in_middle
-    def _():
-        dispatch(order[2], 1, x_middle[2])
-
-    serve_up(order[1])
-
-    @at_end
-    def _():
-        dispatch(order[2], 2)
-
-    serve_down(order[1], is_end)
-
-    @at_end
-    def _():
-        dispatch(order[2], 3)
-        for c in every:
-            combine(1, c, order[1])
-
-    @in_middle
-    def _():
-        for c in range(2, pieces):
-            dispatch(order[2], c, x_middle[2])
         for c in range(lead, pieces):
-            x_copy(0, z, c, outer_z).start()
+            x_copy(2, z, c, outer_z).start()
         for c in every:
             send_all(ret, order[1], c)
         for c in every:
             hold(0, c)
-
-    serve_up(order[2])
-    serve_down(order[2], True)
-
-    @at_end
-    def _():
-        for c in every:
-            combine(2, c, slot_from(order[2], 1 - low_half))
-        for c in every:
-            finish(c, (slot_from(z, low_half),))
-        for c in every:
-            x_copy(1, z, c, inner_z).wait_send()
-
-    @in_middle
-    def _():
-        to_middle = slot_from(order[0], 1 - low_half)
-        to_end = slot_from(order[1], low_half)
-        for c in every:
-            send_all(ret, z, c)
-        relay(0, 0, to_middle, inner_z)
-        for c in every:
-            hold(1, c)
-        relay(0, 1, to_middle, inner_z)
-        relay(0, 2, to_middle, inner_z)
-        hold(2, 0)
-        hold(2, 1)
-        relay(0, 3, to_middle, inner_z)
-        hold(2, 2)
-        hold(2, 3)
-        relay(2, 0, order[2], inner_z)
-        for c in every:
-            combine_own(c)
-        for c in range(1, pieces + 1):
-            if c < pieces:
-                relay(2, c, order[2], inner_z)
-            relay(1, c - 1, to_end, outer_z)
-        for c in every:
-            finish(c, (z, DEPTH))
-        for c in every:
-            for k, level in enumerate((outer_z, inner_z)):
-                x_copy(k, z, c, level).wait_send()
-            for j in range(DEPTH - 1):
-                x_copy(0, order[j], c, x_middle[j]).wait_send()
 
     @pl.when(has_next)
     def _():
@@ -574,22 +594,63 @@
         def _():
             conv_copy(b, tp).wait_send()
 
-    for i in range(DEPTH - 1):
-        meta_copy(i).wait_send()
-
-    @pl.loop(0, DEPTH)
-    def _(s):
-        @pl.loop(0, pieces)
-        def _(c):
-            everyone(*go, s, c).wait_send()
-            everyone(*ret, s, c).wait_send()
-
-            @pl.when(s != z)
-            def _():
-                part_copy(s, c, s, inner_z).wait_send()
-
-
-def run_layer(front, routing, gate_proj, up_proj, down_proj, out_proj, cap, pieces=4):
+    meta_copy(0, z, inner_z).wait_send()
+
+    @pl.when(inward > 0)
+    def _():
+        meta_copy(1, z, outer_z).wait_send()
+        for j in range(DEPTH - 1):
+            meta_copy(2 + j, order[j], x_middle[j]).wait_send()
+
+    serve_up(order[2], hooks({4: then(hand_on, 1, 4), 6: then(hand_on, 1, 5)}, {}))
+    serve_down(order[2], True, hooks({3: then(hand_on, 1, 6), 7: then(hand_on, 1, 7)}, {}))
+
+    @at_end
+    def _():
+        for c in range(pieces - 4, pieces):
+            send_all(ret, z, c)
+        for c in every:
+            combine(2, c, slot_from(order[2], 1 - low_half))
+        for c in every:
+            combine_own(c)
+        slots_sent()
+        for c in every:
+            finish(c, (slot_from(z, low_half),))
+
+    @in_middle
+    def _():
+        to_middle = slot_from(order[0], 1 - low_half)
+        to_end = slot_from(order[1], low_half)
+        for c in every:
+            send_all(ret, z, c)
+        relay(0, 0, to_middle, inner_z)
+        relay(0, 1, to_middle, inner_z)
+        for c in every:
+            hold(1, c)
+        relay(0, 2, to_middle, inner_z)
+        relay(0, 3, to_middle, inner_z)
+        for c in range(4, pieces):
+            relay(0, c, to_middle, inner_z)
+            hold(2, 2 * c - 8)
+            hold(2, 2 * c - 7)
+        relay(2, 0, order[2], inner_z)
+        for c in every:
+            combine_own(c)
+        for c in range(1, pieces + 2):
+            if c < pieces:
+                relay(2, c, order[2], inner_z)
+            if c >= 2:
+                relay(1, c - 2, to_end, outer_z)
+        slots_sent()
+        all_sent(x_all.at[pl.ds(0, DEPTH - 1)], x_send.at[0])
+        all_sent(x_all.at[0], x_send.at[2])
+        for c in every:
+            finish(c, (z, DEPTH))
+
+    all_sent(part_out.at[pl.ds(0, DEPTH - 1)], part_send.at[0])
+
+
+def run_layer(front, routing, gate_proj, up_proj, down_proj, out_proj, cap, pieces=8):
     sp_count, tp_count = lax.axis_size("sp"), lax.axis_size("tp")
     length, channels = front[0].shape
     lanes = front[4].shape[1]
@@ -607,7 +668,7 @@
     arrays = (*front, *routing)
     return pl.pallas_call(
         functools.partial(layer_kernel, sp_count, tp_count, cap, pieces),
-        out_shape=jax.ShapeDtypeStruct((rows, width), bf16),
+        out_shape=pltpu.VMEM((rows, width), bf16),
         in_specs=[hbm] * (len(arrays) + 4),
         out_specs=pl.BlockSpec(memory_space=pltpu.VMEM),
         scratch_shapes=[vmem(a.shape, a.dtype) for a in arrays]
@@ -647,15 +708,15 @@
             dma((tp_count,)),
             dma((tp_count,)),
             dma((tp_count,)),
-            dma((DEPTH - 1,)),
+            dma((DEPTH + 1,)),
             dma((DEPTH,)),
-            dma((2, DEPTH, pieces)),
+            dma((3,)),
             dma((DEPTH, pieces)),
+            dma((1,)),
             dma((DEPTH, pieces)),
+            dma((1,)),
             dma((DEPTH, pieces)),
-            dma((DEPTH, pieces)),
-            dma((DEPTH, pieces)),
-            dma((DEPTH, pieces)),
+            dma((1,)),
             dma((DEPTH + 1, pieces)),
         ],
         compiler_params=pltpu.CompilerParams(

time: 81.7 us -> 76 us (0.930)
  Pallas kernels: 79.7 us -> 75.1 us
  local copies, waits for them, and re-layouts: 1.88 us -> 0.8 us
    pallas_call x1, Pallas kernels: 79.7 us -> 75.1 us  [run_layer(): pl.pallas_call(functools.partial(layer_kernel, sp_count, tp_count, cap, p...]
    unnamed x1, local copies, waits for them, and re-layouts: 1.88 us -> 0.8 us
where the time goes in v3:
time: 76 us; the launch traced here: 75.9 us
  Pallas kernels  75.1 us (99%)
  local copies, waits for them, and re-layouts  0.8 us (1%)
    pallas_call x1, Pallas kernels, run_layer(): pl.pallas_call(functools.partial(layer_kernel, sp_count, tp_count, cap, p...  75.1 us

profile of v3, /device:TPU:0, one launch (start us, length us, event | category | flops | bytes accessed | tf_op | source)
XLA Modules:
  0.0 75.9 jit_solution(5502644108796128754)
XLA Ops:
  0.0 75.1 %shard_map.127 = bf16[128,2048]{1,0:T(8,128)(2,1)S(1)} custom-call(bf16[512,256]{1,0:T(8,128)(2,1)} %conv_hbm.1, bf16[512,256]{1,0:T(8,128)(2,1)} %inner_hbm.1, bf16[512,256]{1,0:T(8,128)(2,1)} %outer_hbm.1, bf16[3,256]{1,0:T(4,128)(2,1)} %taps_hbm.1, s32[4,128]{1,0:T(4,128)} %bitcast.5, bf16[128,2048]{1,0:T(8,128)(2,1)} %residual_hbm.1, f32[1,2048]{1,0:T(1,128)} %bitcast.4, ...), custom_call_target="tpu_custom_call" | custom-call | tf_op jit(solution)/shard_map/pallas_call | solution.py:669
  75.1 0.8 %copy.15 = bf16[128,2048]{1,0:T(8,128)(2,1)} copy(bf16[128,2048]{1,0:T(8,128)(2,1)S(1)} %shard_map.127) | data formatting | bytes 1048576

commit v4 on v3

--- a/solution.py
+++ b/solution.py
@@ -529,35 +529,32 @@
 
     @at_end
     def _():
-        for c in range(3, 6):
+        for c in range(3, pieces):
             hand_on(0, c - 3)
             arrive(1, c)
-            send_back(0, c + 2)
-        hand_on(0, 3)
-        arrive(1, 6)
-        hand_on(0, 4)
-        arrive(1, 7)
+            if c == 3:
+                send_back(0, 5)
+        send_back(0, 6, 7)
         hand_on(0, 5)
 
     serve_up(
         order[1],
         hooks(
-            {3: then(hand_on, 0, 6), 5: then(hand_on, 0, 7)},
+            {3: then(arrive, 2, 2), 6: then(arrive, 2, 3)},
             {1: then(pass_on, 2, 5), 7: then(pass_on, 2, 6)},
         ),
     )
-
     serve_down(
         order[1],
         None,
         hooks(
             {
-                0: then(send_back, 1, 0),
-                1: both(then(send_back, 1, 1), then(arrive, 2, 2)),
-                2: then(send_back, 1, 2),
-                3: both(then(send_back, 1, 3), then(arrive, 2, 3)),
-                5: then(arrive, 2, 4),
-                7: then(arrive, 2, 5),
+                0: both(then(send_back, 1, 0), then(hand_on, 0, 6)),
+                1: both(then(arrive, 2, 4), then(send_back, 1, 1)),
+                2: both(then(send_back, 1, 2), then(hand_on, 0, 7)),
+                3: then(send_back, 1, 3),
+                5: then(arrive, 2, 5),
+                7: then(send_back, 1, 4),
             },
             {3: then(pass_on, 2, 7)},
         ),
@@ -566,7 +563,7 @@
     @at_end
     def _():
         arrive(2, 6)
-        send_back(1, 4, 5)
+        send_back(1, 5)
         hand_on(1, 0)
         arrive(2, 7)
         send_back(1, 6, 7)
@@ -602,8 +599,28 @@
         for j in range(DEPTH - 1):
             meta_copy(2 + j, order[j], x_middle[j]).wait_send()
 
-    serve_up(order[2], hooks({4: then(hand_on, 1, 4), 6: then(hand_on, 1, 5)}, {}))
-    serve_down(order[2], True, hooks({3: then(hand_on, 1, 6), 7: then(hand_on, 1, 7)}, {}))
+    to_middle = slot_from(order[0], 1 - low_half)
+    to_end = slot_from(order[1], low_half)
+
+    def add_on(j, *cs):
+        for c in cs:
+            relay(j, c, to_middle, inner_z)
+
+    serve_up(
+        order[2],
+        hooks(
+            {4: then(hand_on, 1, 4), 6: then(hand_on, 1, 5)},
+            {0: then(add_on, 0, 0), 4: then(add_on, 0, 1)},
+        ),
+    )
+    serve_down(
+        order[2],
+        True,
+        hooks(
+            {3: then(hand_on, 1, 6), 7: then(hand_on, 1, 7)},
+            {1: then(add_on, 0, 2), 5: then(add_on, 0, 3)},
+        ),
+    )
 
     @at_end
     def _():
@@ -619,28 +636,25 @@
 
     @in_middle
     def _():
-        to_middle = slot_from(order[0], 1 - low_half)
-        to_end = slot_from(order[1], low_half)
         for c in every:
             send_all(ret, z, c)
-        relay(0, 0, to_middle, inner_z)
-        relay(0, 1, to_middle, inner_z)
+        add_on(0, 4)
         for c in every:
             hold(1, c)
-        relay(0, 2, to_middle, inner_z)
-        relay(0, 3, to_middle, inner_z)
-        for c in range(4, pieces):
-            relay(0, c, to_middle, inner_z)
-            hold(2, 2 * c - 8)
-            hold(2, 2 * c - 7)
+        add_on(0, 5, 6)
+        for c in every:
+            hold(2, c)
+            if c == 2:
+                add_on(0, 7)
         relay(2, 0, order[2], inner_z)
-        for c in every:
-            combine_own(c)
-        for c in range(1, pieces + 2):
-            if c < pieces:
-                relay(2, c, order[2], inner_z)
-            if c >= 2:
-                relay(1, c - 2, to_end, outer_z)
+        for c in range(1, pieces):
+            relay(2, c, order[2], inner_z)
+            if c >= 4:
+                relay(1, c - 4, to_end, outer_z)
+            combine_own(c - 1)
+        combine_own(pieces - 1)
+        for c in range(pieces - 4, pieces):
+            relay(1, c, to_end, outer_z)
         slots_sent()
         all_sent(x_all.at[pl.ds(0, DEPTH - 1)], x_send.at[0])
         all_sent(x_all.at[0], x_send.at[2])

time: 76 us -> 72.8 us (0.958)
  Pallas kernels: 75.1 us -> 71.8 us
    pallas_call x1, Pallas kernels: 75.1 us -> 71.8 us  [run_layer(): pl.pallas_call(functools.partial(layer_kernel, sp_count, tp_count, cap, p...]
where the time goes in v4:
time: 72.8 us; the launch traced here: 72.6 us
  Pallas kernels  71.8 us (99%)
  local copies, waits for them, and re-layouts  0.8 us (1%)
    pallas_call x1, Pallas kernels, run_layer(): pl.pallas_call(functools.partial(layer_kernel, sp_count, tp_count, cap, p...  71.8 us

profile of v4, /device:TPU:0, one launch (start us, length us, event | category | flops | bytes accessed | tf_op | source)
XLA Modules:
  0.0 72.6 jit_solution(12129156645381089214)
XLA Ops:
  0.0 71.8 %shard_map.127 = bf16[128,2048]{1,0:T(8,128)(2,1)S(1)} custom-call(bf16[512,256]{1,0:T(8,128)(2,1)} %conv_hbm.1, bf16[512,256]{1,0:T(8,128)(2,1)} %inner_hbm.1, bf16[512,256]{1,0:T(8,128)(2,1)} %outer_hbm.1, bf16[3,256]{1,0:T(4,128)(2,1)} %taps_hbm.1, s32[4,128]{1,0:T(4,128)} %bitcast.5, bf16[128,2048]{1,0:T(8,128)(2,1)} %residual_hbm.1, f32[1,2048]{1,0:T(1,128)} %bitcast.4, ...), custom_call_target="tpu_custom_call" | custom-call | tf_op jit(solution)/shard_map/pallas_call | solution.py:683
  71.8 0.8 %copy.15 = bf16[128,2048]{1,0:T(8,128)(2,1)} copy(bf16[128,2048]{1,0:T(8,128)(2,1)S(1)} %shard_map.127) | data formatting | bytes 1048576

commit v5 on v4

--- a/solution.py
+++ b/solution.py
@@ -21,7 +21,7 @@
     padded, padded_docs, tail, tail_in, fix, fix_in, conv_out, conv_in, carried_ref,
     metas, place, wide, high, low, x_all, slots, arrived, served, back, hidden, sums, held, part_out, part_in,
     load_sem, tail_send, tail_recv, fix_send, fix_recv, conv_send, conv_recv, meta_send, meta_recv, x_send, x_recv,
-    go_send, go_recv, ret_send, ret_recv, part_send, part_recv,
+    go_send, go_recv, ret_send, part_send, part_recv,
 ):
     sp = lax.axis_index("sp")
     tp = lax.axis_index("tp")
@@ -314,7 +314,7 @@
         )
 
     go = (slots, arrived, go_send, go_recv)
-    ret = (served, back, ret_send, ret_recv)
+    ret = (served, back, ret_send, x_recv)
 
     def send_all(way, s, c):
         for n in range(group - 1):
@@ -540,7 +540,7 @@
     serve_up(
         order[1],
         hooks(
-            {3: then(arrive, 2, 2), 6: then(arrive, 2, 3)},
+            {3: then(arrive, 2, 2)},
             {1: then(pass_on, 2, 5), 7: then(pass_on, 2, 6)},
         ),
     )
@@ -550,7 +550,7 @@
         hooks(
             {
                 0: both(then(send_back, 1, 0), then(hand_on, 0, 6)),
-                1: both(then(arrive, 2, 4), then(send_back, 1, 1)),
+                1: both(then(arrive, 2, 3, 4), then(send_back, 1, 1)),
                 2: both(then(send_back, 1, 2), then(hand_on, 0, 7)),
                 3: then(send_back, 1, 3),
                 5: then(arrive, 2, 5),
@@ -729,7 +729,6 @@
             dma((1,)),
             dma((DEPTH, pieces)),
             dma((1,)),
-            dma((DEPTH, pieces)),
             dma((1,)),
             dma((DEPTH + 1, pieces)),
         ],

time: 72.8 us -> 73.2 us (level)
  no operation moved by 1% of the time
where the time goes in v5:
time: 73.2 us; the launch traced here: 73 us
  Pallas kernels  72.2 us (99%)
  local copies, waits for them, and re-layouts  0.8 us (1%)
    pallas_call x1, Pallas kernels, run_layer(): pl.pallas_call(functools.partial(layer_kernel, sp_count, tp_count, cap, p...  72.2 us

profile of v5, /device:TPU:0, one launch (start us, length us, event | category | flops | bytes accessed | tf_op | source)
XLA Modules:
  0.0 73.0 jit_solution(15358113896125091804)
XLA Ops:
  0.0 72.2 %shard_map.127 = bf16[128,2048]{1,0:T(8,128)(2,1)S(1)} custom-call(bf16[512,256]{1,0:T(8,128)(2,1)} %conv_hbm.1, bf16[512,256]{1,0:T(8,128)(2,1)} %inner_hbm.1, bf16[512,256]{1,0:T(8,128)(2,1)} %outer_hbm.1, bf16[3,256]{1,0:T(4,128)(2,1)} %taps_hbm.1, s32[4,128]{1,0:T(4,128)} %bitcast.5, bf16[128,2048]{1,0:T(8,128)(2,1)} %residual_hbm.1, f32[1,2048]{1,0:T(1,128)} %bitcast.4, ...), custom_call_target="tpu_custom_call" | custom-call | tf_op jit(solution)/shard_map/pallas_call | solution.py:683
  72.2 0.8 %copy.15 = bf16[128,2048]{1,0:T(8,128)(2,1)} copy(bf16[128,2048]{1,0:T(8,128)(2,1)S(1)} %shard_map.127) | data formatting | bytes 1048576
